TPU v7x, 256 devices: a whole 4x4x8 slice. The times are simulated.
256 devices in a mesh: sp: 64 (over z, y, core), tp: 4 (over x).
Axes of the slice: x: 4, y: 4, z: 8, core: 2. Of those that a mesh axis runs over, the one named last changes fastest.
Arguments:
- tokens_in: bfloat16 [16384, 2048], P('sp'), may hold values from -3 to 3
- queries: bfloat16 [16384, 1024], P('sp', 'tp'), may hold values from -6 to 6
- keys: bfloat16 [16384, 256], P('sp', 'tp'), may hold values from -6 to 6
- values: bfloat16 [16384, 256], P('sp', 'tp'), may hold values from -12 to 12
- doc_ids: int32 [16384], P('sp'), may hold values from 0 to 15, never falling along the last dimension, each value on 1 to 8448 neighbouring positions
- query_gain: float32 [64], replicated, may hold values from 2.5 to 6
- key_norm_scale: float32 [64], replicated, may hold values from 2.5 to 6
- out_weight: bfloat16 [1024, 2048], P('tp'), may hold values from -0.1875 to 0.1875
- norm_gain: float32 [2048], replicated, may hold values from 0.1 to 1.9
- gate_weight: bfloat16 [2048, 5632], P('sp', 'tp'), may hold values from -0.125 to 0.125
- up_weight: bfloat16 [2048, 5632], P('sp', 'tp'), may hold values from -0.125 to 0.125
- down_weight: bfloat16 [5632, 2048], P('tp', 'sp'), may hold values from -0.078125 to 0.078125
Outputs:
- layer_out: bfloat16 [16384, 2048], P('sp')
Inputs may be any that keep to these rules, and one draw needn't show every extreme that they name: `doc_ids`: document numbers never fall along the sequence; every document has 1 to 8448 positions and one has exactly 8448.
All inputs are finite; a program needn't handle non-finite values.
Results may differ from a plain program's by a relative error of at most 0.014.
The roundings to bfloat16 on the way count: a program that leaves them out, or rounds other values in their place, can miss the bound.
Values may be sent and summed in bfloat16 or wider, within the bound.
A program may use at most 128 MiB of HBM per device.

v0:
```python
import jax
import jax.numpy as jnp
from jax import lax
from jax.sharding import PartitionSpec as P

GRID = 64


EPS = 1e-06
THETA = 10000.0
NEG = -1e30


def in_one_piece(arrays, axis, dim, along):
    ends, at = ([], 0)
    for a in arrays[:-1]:
        at += a.shape[along]
        ends.append(at)
    both = jnp.concatenate(arrays, axis=along)
    return tuple(jnp.split(lax.all_gather(both, axis, axis=dim, tiled=True), ends, axis=along))


def sent_to_all(array, axis):
    copies = jnp.broadcast_to(array, (lax.axis_size(axis), *array.shape))
    return lax.all_to_all(copies, axis, split_axis=0, concat_axis=0, tiled=True)


def of_everyone(array, axis):
    everything = sent_to_all(array, axis)
    return jnp.sum(everything.astype(jnp.float32), axis=0)


def rotate_half(block, angle):
    half_dim = block.shape[-1] // 2
    cosine = jnp.cos(angle)[:, None, :]
    sine = jnp.sin(angle)[:, None, :]
    first = block[..., :half_dim]
    second = block[..., half_dim:]
    return jnp.concatenate(
        [first * cosine - second * sine, second * cosine + first * sine], axis=-1
    )


def normalized_rotated(values_in, gain, heads, lattice_row, lattice_column):
    full = values_in.astype(jnp.float32).reshape(values_in.shape[0], heads, -1)
    full = full * lax.rsqrt(jnp.mean(full * full, axis=-1, keepdims=True) + EPS) * gain
    half_dim = full.shape[-1] // 2
    freqs = THETA ** (-2.0 * jnp.arange(half_dim // 2, dtype=jnp.float32) / half_dim)
    by_row = rotate_half(full[..., :half_dim], lattice_row[:, None] * freqs[None, :])
    by_col = rotate_half(full[..., half_dim:], lattice_column[:, None] * freqs[None, :])
    return jnp.concatenate([by_row, by_col], axis=-1).astype(jnp.bfloat16)


def per_device(
    tokens_in,
    queries,
    keys,
    values,
    doc_ids,
    query_gain,
    key_norm_scale,
    out_weight,
    norm_gain,
    gate_weight,
    up_weight,
    down_weight,
):
    tok_rows = tokens_in.shape[0]
    head_dim = query_gain.shape[0]
    local_heads = queries.shape[1] // head_dim
    places = lax.axis_index("sp") * tok_rows + jnp.arange(tok_rows, dtype=jnp.int32)
    lattice_row = (places // GRID).astype(jnp.float32)
    lattice_column = (places % GRID).astype(jnp.float32)
    q_local = normalized_rotated(queries, query_gain, local_heads, lattice_row, lattice_column)
    q_rows = q_local.transpose(1, 0, 2).reshape(local_heads * tok_rows, head_dim)
    key_pairs = normalized_rotated(keys, key_norm_scale, 1, lattice_row, lattice_column).reshape(
        tok_rows // 2, 2 * head_dim
    )
    value_pairs = values.reshape(tok_rows // 2, 2 * head_dim)
    doc_pairs = doc_ids.reshape(tok_rows // 2, 2)
    row_docs = jnp.tile(doc_ids, local_heads)
    first_doc = doc_ids[0]
    last_doc = doc_ids[-1]
    scale = head_dim ** (-0.5)
    total_rows = local_heads * tok_rows

    def absorb_block(state, key_block, value_block, doc_block):

        def absorb(current):
            running_max, running_sum, running_acc = current
            scores = (
                jnp.einsum("qd,kd->qk", q_rows, key_block, preferred_element_type=jnp.float32)
                * scale
            )
            same = row_docs[:, None] == doc_block[None, :]
            scores = jnp.where(same, scores, NEG)
            new_max = jnp.maximum(running_max, jnp.max(scores, axis=1))
            weights = jnp.where(same, jnp.exp(scores - new_max[:, None]), 0.0)
            shrink = jnp.exp(running_max - new_max)
            new_sum = running_sum * shrink + jnp.sum(weights, axis=1)
            new_acc = running_acc * shrink[:, None] + jnp.dot(
                weights.astype(jnp.bfloat16), value_block, preferred_element_type=jnp.float32
            )
            return (new_max, new_sum, new_acc)

        touches = (doc_block[0] <= last_doc) & (doc_block[-1] >= first_doc)
        return lax.cond(touches, absorb, lambda current: current, state)

    initial = (
        jnp.full((total_rows,), NEG, jnp.float32),
        jnp.zeros((total_rows,), jnp.float32),
        jnp.zeros((total_rows, head_dim), jnp.float32),
    )
    carry = initial
    key_piece, value_piece, doc_piece = (
        *in_one_piece((key_pairs, value_pairs), "sp", 0, 1),
        lax.all_gather(doc_pairs, "sp", axis=0, tiled=True),
    )
    shards = key_piece.shape[0] * 2 // tok_rows
    joined = 1
    while joined * 2 <= shards and shards % (joined * 2) == 0 and (joined * 2 * tok_rows <= 1024):
        joined = joined * 2
    blocks = shards // joined
    span_rows = joined * tok_rows
    key_blocks = key_piece.reshape(blocks, span_rows, head_dim)
    value_blocks = value_piece.reshape(blocks, span_rows, head_dim)
    doc_blocks = doc_piece.reshape(blocks, span_rows)

    def visit(state, inputs):
        key_block, value_block, doc_block = inputs
        return (absorb_block(state, key_block, value_block, doc_block), None)

    carry, unused = lax.scan(visit, carry, (key_blocks, value_blocks, doc_blocks))
    attended = (carry[2] / carry[1][:, None]).astype(jnp.bfloat16)
    attended = (
        attended.reshape(local_heads, tok_rows, head_dim)
        .transpose(1, 0, 2)
        .reshape(tok_rows, local_heads * head_dim)
    )
    partial_value = jnp.dot(attended, out_weight, preferred_element_type=jnp.float32)
    mixed = of_everyone(
        partial_value.astype(jnp.bfloat16).astype(jnp.float32).astype(jnp.bfloat16), "tp"
    ).astype(jnp.float32)
    resid = tokens_in.astype(jnp.float32) + mixed
    normed = (
        resid * lax.rsqrt(jnp.mean(resid * resid, axis=-1, keepdims=True) + EPS) * norm_gain
    ).astype(jnp.bfloat16)
    pieces = in_one_piece((gate_weight, up_weight), "sp", 0, 1)
    gate = jnp.dot(normed, pieces[0], preferred_element_type=jnp.float32)
    up_val = jnp.dot(normed, pieces[1], preferred_element_type=jnp.float32)
    hidden = (jax.nn.silu(gate) * up_val).astype(jnp.bfloat16)
    fed_part = jnp.dot(
        hidden,
        lax.all_gather(down_weight, "sp", axis=1, tiled=True),
        preferred_element_type=jnp.float32,
    )
    fed = of_everyone(
        fed_part.astype(jnp.bfloat16).astype(jnp.float32).astype(jnp.bfloat16), "tp"
    ).astype(jnp.float32)
    return (resid + fed).astype(jnp.bfloat16)


def solution(mesh):
    return jax.shard_map(
        per_device,
        mesh=mesh,
        in_specs=(
            P("sp", None),
            P("sp", "tp"),
            P("sp", "tp"),
            P("sp", "tp"),
            P("sp"),
            P(),
            P(),
            P("tp", None),
            P(),
            P("sp", "tp"),
            P("sp", "tp"),
            P("tp", "sp"),
        ),
        out_specs=P("sp", None),
        check_vma=False,
    )
```

profile of v0, /device:TPU:1, one launch (start us, length us, event | category | flops | bytes accessed | tf_op | source)
XLA Modules:
  0.0 334.5 jit_solution(17414294157486379269)
XLA Ops:
  6.6 0.9 fusion.35
  7.5 0.8 fusion.37
  8.3 0.2 fusion.51
  8.5 0.1 copy.23
  8.6 0.1 convert_element_type.69
  8.7 0.9 copy.24
  9.6 0.1 reshape.321
  9.7 0.6 pad_maximum_fusion.1
  10.4 0.0 all-gather.6.cloned.1.call-start
  10.4 1.6 pad_maximum_fusion
  12.1 0.7 all-gather.8.cloned.1.call-update
  12.8 1.0 copy.25
  13.9 0.2 multiply_cosine_fusion.1
  14.1 0.7 fusion.34
  14.9 0.2 copy.29
  15.1 0.8 reshape.319
  15.9 63.4 %all_gather.12 = s32[8192,2]{1,0:T(8,128)} all-gather(s32[128,2]{1,0:T(8,128)S(1)} %reshape.319), channel_id=1, replica_groups=mesh['sp'=64,'tp'=4] {'sp'}, dimensions={0}, use_global_device_ids=true | all-gather | bytes 66560 | tf_op jit(solution)/shard_map/all_gather | solution.py:117
  79.3 4.0 %reshape.320 = s32[16,1024]{1,0:T(8,128)S(1)} reshape(s32[8192,2]{1,0:T(8,128)} %all_gather.12) | data formatting | bytes 131072 | tf_op jit(solution)/shard_map/reshape | solution.py:127
  83.4 0.7 fusion.60
  84.0 10.1 %all-gather.4.cloned.1.call-done = bf16[8192,256]{1,0:T(8,128)(2,1)} async-done(((bf16[128,256]{1,0:T(8,128)(2,1)}), bf16[8192,256]{1,0:T(8,128)(2,1)}) %all-gather.4.cloned.1.call-update) | async-done | bytes 4194320 | tf_op jit(solution)/shard_map/all_gather | solution.py:20
  94.1 3.9 %fusion.59 = (bf16[8192,128]{1,0:T(8,128)(2,1)S(1)}, bf16[8192,128]{1,0:T(8,128)(2,1)}) fusion(bf16[8192,256]{1,0:T(8,128)(2,1)} %all-gather.4.cloned.1.call-done), kind=kLoop, calls=%fused_computation.96 | loop fusion | bytes 8388608 | tf_op jit(solution)/shard_map/split | solution.py:20
  98.0 6.1 %reshape.322 = bf16[16,1024,64]{2,1,0:T(8,128)(2,1)} reshape(bf16[8192,128]{1,0:T(8,128)(2,1)} %get-tuple-element.229) | data formatting | bytes 4194304 | tf_op jit(solution)/shard_map/reshape | solution.py:125
  104.1 3.3 %reshape.326 = bf16[16,1024,64]{2,1,0:T(8,128)(2,1)} reshape(bf16[8192,128]{1,0:T(8,128)(2,1)S(1)} %get-tuple-element.228) | data formatting | bytes 4194304 | tf_op jit(solution)/shard_map/reshape | solution.py:126
  107.5 60.9 %while.15 = (s32[]{:T(128)}, f32[1024]{0:T(1024)S(1)}, f32[1024]{0:T(1024)S(1)}, f32[1024,64]{0,1:T(8,128)S(1)}, s32[16,1024]{1,0:T(8,128)S(1)}, /*index=5*/s32[...) while((s32[]{:T(128)}, f32[1024]{0:T(1024)S(1)}, ...), condition=%wide.region_7.8_spmd.clone, body=%wide.region_2.7_spmd.clone.sunk | while | flops 285345792 | bytes 13875527 | solution.py:133
  107.5 0.6 fusion.68
  110.6 5.5 %conditional.3 = ((f32[1024]{0:T(1024)S(1)}, f32[1024]{0:T(1024)S(1)}, f32[1024,64]{0,1:T(8,128)S(1)})) conditional(s32[]{:T(128)} %convert_element_type.111, (f32[1024]{0:T(1024)S(1)}, f32[1024]{0:T(1024)S(1)}, f32[1024,64]{0,1:T(8,128)S(1)}) %tuple.58, (s32[256]{0:T(256)S(1)}, s32[1,1024]{1,0:T(1,128)S(1)}, bf16[16,1024,64]{2,1,0:T(8,128)(2,1)}, ...), branch_computations={%region_3.3_spmd, %region_4.6_spmd} | conditional | flops 285345792 | bytes 13867040 | solution.py:107
  110.6 1.7 fusion.2
  112.4 1.5 fusion.4
  113.9 2.2 fusion.7
  116.1 0.6 fusion.68
  119.2 5.5 %conditional.3 = ((f32[1024]{0:T(1024)S(1)}, f32[1024]{0:T(1024)S(1)}, f32[1024,64]{0,1:T(8,128)S(1)})) conditional(s32[]{:T(128)} %convert_element_type.111, (f32[1024]{0:T(1024)S(1)}, f32[1024]{0:T(1024)S(1)}, f32[1024,64]{0,1:T(8,128)S(1)}) %tuple.58, (s32[256]{0:T(256)S(1)}, s32[1,1024]{1,0:T(1,128)S(1)}, bf16[16,1024,64]{2,1,0:T(8,128)(2,1)}, ...), branch_computations={%region_3.3_spmd, %region_4.6_spmd} | conditional | flops 285345792 | bytes 13867040 | solution.py:107
  119.2 1.7 fusion.2
  121.0 1.5 fusion.4
  122.5 2.2 fusion.7
  124.7 0.6 fusion.68
  127.9 0.6 fusion.68
  131.0 0.6 fusion.68
  134.1 0.6 fusion.68
  137.2 0.6 fusion.68
  140.4 0.6 fusion.68
  143.5 0.6 fusion.68
  146.6 0.6 fusion.68
  149.7 0.6 fusion.68
  152.8 0.6 fusion.68
  156.0 0.6 fusion.68
  159.1 0.6 fusion.68
  162.2 0.6 fusion.68
  165.3 0.6 fusion.68
  168.5 0.1 reshape.327
  168.6 0.5 convolution_convert_fusion
  169.1 0.5 broadcast_in_dim.23
  169.6 48.4 %all_to_all.10 = bf16[4,256,2048]{2,1,0:T(8,128)(2,1)S(1)} all-to-all(bf16[4,256,2048]{2,1,0:T(8,128)(2,1)S(1)} %broadcast_in_dim.23), channel_id=1, replica_groups=mesh['sp'=64,'tp'=4] {'tp'}, dimensions={0} | all-to-all | bytes 8388608 | tf_op jit(solution)/shard_map/all_to_all | solution.py:25
  218.0 0.8 convert_reduce_fusion.1
  218.8 0.4 copy-done.1
  219.2 0.4 multiply_reduce_fusion
  219.6 1.3 multiply_convert_fusion
  221.0 5.9 %fusion.22 = f32[256,1408]{1,0:T(8,128)} fusion(bf16[256,2048]{1,0:T(8,128)(2,1)} %multiply_convert_fusion, bf16[2048,2816]{1,0:T(8,128)(2,1)} %all-gather.6.cloned.1.call-done), kind=kOutput, calls=%fused_computation.27 | convolution fusion | flops 1476395008 | bytes 8257536 | tf_op jit(solution)/shard_map/dot_general | solution.py:149
  226.9 35.0 %all-gather.8.cloned.1.call-done = bf16[1408,2048]{0,1:T(8,128)(2,1)} async-done(((bf16[1408,32]{0,1:T(8,128)(2,1)}), bf16[1408,2048]{0,1:T(8,128)(2,1)}) %all-gather.8.cloned.1.call-update) | async-done | bytes 5767184 | tf_op jit(solution)/shard_map/all_gather | solution.py:154
  261.9 9.5 %convolution_convert_fusion.1 = bf16[256,2048]{1,0:T(8,128)(2,1)} fusion(bf16[1408,2048]{0,1:T(8,128)(2,1)} %all-gather.8.cloned.1.call-done, bf16[256,2048]{1,0:T(8,128)(2,1)} %multiply_convert_fusion, bf16[2048,2816]{1,0:T(8,128)(2,1)} %all-gather.6.cloned.1.call-done, f32[256,1408]{1,0:T(8,128)} %fusion.22), kind=kOutput, calls=%fused_computation.32 | convolution fusion | flops 2955476992 | bytes 15073280 | tf_op jit(solution)/shard_map/dot_general | solution.py:152
  271.4 1.7 broadcast_in_dim.24
  273.1 52.1 %all_to_all.11 = bf16[4,256,2048]{2,1,0:T(8,128)(2,1)S(1)} all-to-all(bf16[4,256,2048]{2,1,0:T(8,128)(2,1)S(1)} %broadcast_in_dim.24), channel_id=1, replica_groups=mesh['sp'=64,'tp'=4] {'tp'}, dimensions={0} | all-to-all | bytes 8388608 | tf_op jit(solution)/shard_map/all_to_all | solution.py:25
  325.3 0.8 convert_reduce_fusion
  326.1 0.4 copy-done.2
  326.5 1.5 add_convert_fusion
  (67 shorter events, 0.7 us)
Async XLA Ops:
  6.5 162.0 %copy-start = (bf16[256,2048]{1,0:T(8,128)(2,1)S(1)}, bf16[256,2048]{1,0:T(8,128)(2,1)}, u32[]{:S(2)}) copy-start(bf16[256,2048]{1,0:T(8,128)(2,1)} %param.23) | copy-start | bytes 3145732
  6.5 87.6 %all-gather.4.cloned.1.call-start = ((), (), s32[]{:S(2)}) async-start(), calls=%async_computation.2 | async-start | bytes 4259840 | tf_op jit(solution)/shard_map/all_gather | solution.py:20
  10.4 210.6 %all-gather.6.cloned.1.call-start = ((), (), s32[]{:S(2)}) async-start(), calls=%async_computation.3 | async-start | bytes 11714560 | tf_op jit(solution)/shard_map/all_gather | solution.py:20
  12.1 249.8 %all-gather.8.cloned.1.call-start = ((), (), s32[]{:S(2)}) async-start(), calls=%async_computation.4 | async-start | bytes 5857280 | tf_op jit(solution)/shard_map/all_gather | solution.py:154
  15.9 67.5 %copy-start.3 = (s32[256]{0:T(256)S(1)}, s32[256]{0:T(256)}, u32[]{:S(2)}) copy-start(s32[256]{0:T(256)} %param.20) | copy-start | bytes 3076
  218.0 1.2 copy-start.1
  218.0 1.6 copy-start.4
  325.3 1.2 copy-start.2
Sparse Core Ops, SparseCore 0:
  10.5 83.5 all-gather.3
  96.9 85.2 all-gather.5
  184.9 76.9 all-gather.7
where the time goes:
time: 339 us; the launch traced here: 335 us
  blocking collectives  164 us (48%)
  waiting for transfers between devices  45.8 us (14%)
  loops' own time  40.4 us (12%)
  local copies, waits for them, and re-layouts  34.1 us (10%)
  matrix products  23.6 us (7%)
  between operations  13.3 us (4%)
  other arithmetic  13.2 us (4%)
    all_to_all x2, blocking collectives, sent_to_all(): return lax.all_to_all(copies, axis, split_axis=0, concat_axis=0, tiled=True)  100 us
    all_gather x1, blocking collectives, per_device(): lax.all_gather(doc_pairs, 'sp', axis=0, tiled=True)  63.4 us
    another operation x1, loops' own time, per_device(): lax.scan(visit, carry, (key_blocks, value_blocks, doc_blocks))  40.1 us
    all_gather x1, waiting for transfers between devices, per_device(): lax.all_gather(down_weight, 'sp', axis=1, tiled=True)  35 us
    all_gather x2, waiting for transfers between devices, in_one_piece(): lax.all_gather(both, axis, axis=dim, tiled=True)  10.1 us
    slice x16, local copies, waits for them, and re-layouts, absorb_block(): touches = (doc_block[0] <= last_doc) & (doc_block[-1] >= first_doc)  9.5 us
    dot_general x1, matrix products, per_device(): jnp.dot(hidden, lax.all_gather(down_weight, 'sp', axis=1, tiled=True), pr...  9.48 us
  transfers between devices with their start and end apart: 3, of which 2 were waited for; matrix products, arithmetic and copies ran while one was open for 16% of the time, Pallas kernels for 0%

commit v1 on v0

v1 whole, which is shorter than its diff:
```python
import heapq
import jax
import jax.numpy as jnp
import numpy as np
from jax import lax
from jax.experimental import pallas as pl
from jax.experimental.pallas import tpu as pltpu
from jax.sharding import PartitionSpec as P

GRID = 64
EPS = 1e-06
THETA = 10000.0
NEG = -1e30
NZ, NY, NC, NX = 8, 4, 2, 4
DZS = (0, 1, -1, 2, -2, 3, -3, 4)
DYS = (0, 1, -1, 2)
MESH = pl.DeviceIdType.MESH
F32, BF16 = jnp.float32, jnp.bfloat16

PARTS = (
    ("k", "zy", 0.88, 0),
    ("v", "yz", 0.70, 0),
    ("g", "zy", 1.93, 1),
    ("u", "yz", 1.93, 1),
    ("a", "zy", 1.58, 2),
    ("b", "yz", 0.35, 2),
)


def spread(order, flip):
    messages = {}

    def z_ring(dy, up):
        for d in (1, 2, 3):
            messages[-d, dy] = ("z+", (-d + 1, dy))
            messages[d, dy] = ("z-", (d - 1, dy))
        messages[4, dy] = ("z+", (-3, dy)) if up else ("z-", (3, dy))

    def y_ring(dz, up):
        messages[dz, -1] = ("y+", (dz, 0))
        messages[dz, 1] = ("y-", (dz, 0))
        messages[dz, 2] = ("y+", (dz, -1)) if up else ("y-", (dz, 1))

    if order == "zy":
        z_ring(0, flip)
        for n, dz in enumerate(sorted(DZS)):
            y_ring(dz, (n + flip) % 2 == 0)
    else:
        y_ring(0, flip)
        for n, dy in enumerate(sorted(DYS)):
            z_ring(dy, (n + flip) % 2 == 0)
    return messages


def plan():
    received = {p[0]: spread(p[1], i % 2) for i, p in enumerate(PARTS)}
    cost = {p[0]: p[2] for p in PARTS}
    prio = {p[0]: p[3] for p in PARTS}
    follow = {}
    for part, messages in received.items():
        for key, (link, held) in messages.items():
            follow.setdefault((part, held), []).append((link, key))

    def depth(part, key):
        return max([1 + depth(part, k) for _, k in follow.get((part, key), [])], default=0)

    now, order = 0.0, []
    link_free = {link: 0.0 for link in ("z+", "z-", "y+", "y-", "d")}
    queues = {link: [] for link in link_free}
    arrivals = []
    have, sib = set(), set()
    latency, count = 2.0, 0

    def got(part, key):
        nonlocal count
        have.add((part, key))
        for link, k in follow.get((part, key), []):
            count += 1
            heapq.heappush(queues[link], (prio[part], -depth(part, k), count, part, k, key))
        dz = key[0]
        if all((part, (dz, dy)) in have for dy in DYS):
            order.append(("sib", part, dz))
            start = max(now, link_free["d"])
            link_free["d"] = start + 0.3
            count += 1
            heapq.heappush(arrivals, (start + 1.5, count, "sib", part, dz))

    def tick():
        nonlocal count
        while arrivals and arrivals[0][0] <= now:
            _, _, kind, part, key = heapq.heappop(arrivals)
            order.append(("wait" + kind, part, key))
            if kind == "sib":
                sib.add((part, key))
            else:
                got(part, key)
        for link in ("z+", "z-", "y+", "y-"):
            q = queues[link]
            while q and link_free[link] - now < 3.0:
                _, _, _, part, key, held = heapq.heappop(q)
                order.append(("send", part, key, held, link))
                start = max(now, link_free[link])
                link_free[link] = start + cost[part]
                count += 1
                heapq.heappush(arrivals, (link_free[link] + latency, count, "", part, key))

    def ready(step):
        kind = step[0]
        if kind == "attend":
            _, dz, own = step
            return all(((p, (dz, dy)) in have for p in "kv" for dy in DYS) if own else ((p, dz) in sib for p in "kv"))
        if kind == "gateup":
            return all((p, (dz, dy)) in have for p in "gu" for dz in DZS for dy in DYS) and all(
                (p, dz) in sib for p in "gu" for dz in DZS
            )
        if kind == "down":
            return all(
                all((p, (dz, dy)) in have for p in "ab" for dy in DYS) and all((p, dz) in sib for p in "ab")
                for dz in DZS[2 * step[1] : 2 * step[1] + 2]
            )
        return True

    steps = [("attend", dz, own) for dz in DZS for own in (True, False)]
    times = {"attend": 2.2, "attended": 1.0, "x_att": 2.5, "x_att2": 2.5, "mix": 1.0, "gateup": 0.9, "down": 0.8}
    steps += [("attended",), ("x_att",), ("x_att2",), ("mix", 0), ("mix", 1)]
    steps += [("gateup", n) for n in range(6)]
    steps += [("down", n) for n in range(4)]
    for part in "kvgu":
        got(part, (0, 0))
    tick()
    order.append(("more",))
    for part in "ab":
        got(part, (0, 0))
    for step in steps:
        tick()
        while not ready(step):
            now = max(now, arrivals[0][0])
            tick()
        order.append(step)
        now += times[step[0]]
    while arrivals:
        now = max(now, arrivals[0][0])
        tick()
    order.append(("end",))
    return order, now, link_free


def turn_tables():
    lane = np.arange(64)
    freqs = THETA ** (-2.0 * (lane % 16) / 32.0)
    sign = np.where(lane % 32 < 16, -1.0, 1.0)
    rows = np.arange(256)[:, None] * freqs[None]
    by_row = lane < 32
    row_cos = np.where(by_row, np.cos(rows), 0.0).reshape(64, 4, 64)
    row_sin = np.where(by_row, np.sin(rows) * sign, 0.0).reshape(64, 4, 64)
    row = np.concatenate([row_cos, row_sin], axis=1)
    cols = np.arange(64)[:, None] * freqs[None]
    col_cos = np.where(by_row, 0.0, np.cos(cols))
    col_sin = np.where(by_row, 0.0, np.sin(cols) * sign)
    col = np.stack([col_cos, col_sin])
    return np.tile(row, (1, 1, 2)).astype(np.float32), np.tile(col, (1, 1, 2)).astype(np.float32)


def nt(a, b):
    return lax.dot_general(a, b, (((1,), (1,)), ((), ())), preferred_element_type=F32)


def nn(a, b):
    return lax.dot_general(a, b, (((1,), (0,)), ((), ())), preferred_element_type=F32)


def kernel(
    tokens_ref,
    q_ref,
    k_ref,
    v_ref,
    doc_ref,
    gains_ref,
    ow_ref,
    ng_ref,
    gate_ref,
    up_ref,
    down_ref,
    row_ref,
    col_ref,
    out_ref,
    kt,
    vt,
    wg,
    wu,
    wa,
    wb,
    ow,
    att,
    qs,
    m_ref,
    l_ref,
    acc_ref,
    s_ref,
    p_ref,
    tok,
    resid,
    normed,
    hidden,
    part_buf,
    rs_buf,
    recv_sem,
    send_sem,
    sib_recv,
    sib_send,
    ow_recv,
    ow_send,
    ow_sib_recv,
    ow_sib_send,
    att_recv,
    att_send,
    rs_recv,
    rs_send,
    ag_recv,
    ag_send,
    local_sem,
):
    s = lax.axis_index("sp")
    x = lax.axis_index("tp")
    c = lax.rem(s, NC)
    y = lax.rem(s // NC, NY)
    z = s // (NC * NY)
    d = 1 - 2 * c

    def wz(dz):
        return lax.rem(z + (dz + NZ), NZ)

    def wy(dy):
        return lax.rem(y + (dy + NY), NY)

    def wx(dx):
        return lax.rem(x + (dx + NX), NX)

    def at(zz, yy, cc, xx):
        return ((zz * NY + yy) * NC + cc, xx)

    neighbour = {
        "z+": at(wz(1), y, c, x),
        "z-": at(wz(-1), y, c, x),
        "y+": at(z, wy(1), c, x),
        "y-": at(z, wy(-1), c, x),
    }
    sibling = at(z, y, 1 - c, x)
    x_plus = at(z, y, c, wx(1))
    x_minus = at(z, y, c, wx(-1))
    x_far = at(z, y, c, wx(2))
    x_f = at(z, y, c, wx(d))
    x_r = at(z, y, c, wx(-d))

    arrays = {"k": kt, "v": vt, "g": wg, "u": wu, "a": wa, "b": wb}
    names = [p[0] for p in PARTS]
    received = {p[0]: spread(p[1], i % 2) for i, p in enumerate(PARTS)}
    index = {name: {key: n for n, key in enumerate(received[name])} for name in names}

    local = [
        pltpu.make_async_copy(gate_ref, wg.at[z, y, c], local_sem.at[0]),
        pltpu.make_async_copy(up_ref, wu.at[z, y, c], local_sem.at[1]),
        pltpu.make_async_copy(ow_ref, ow.at[x], local_sem.at[2]),
        pltpu.make_async_copy(tokens_ref, tok, local_sem.at[3]),
    ]
    for copy in local:
        copy.start()

    barrier = pltpu.get_barrier_semaphore()
    for who in (*neighbour.values(), sibling, x_plus, x_minus, x_far):
        pl.semaphore_signal(barrier, inc=1, device_id=who, device_id_type=MESH)

    lane = lax.broadcasted_iota(jnp.int32, (256, 128), 1)
    low = lane < 64
    swap_up = lax.rem(lane // 16, 2) == 0
    row = row_ref[s]
    cos = jnp.concatenate([jnp.broadcast_to(row[r : r + 1], (64, 128)) + col_ref[0] for r in range(4)], axis=0)
    sin = jnp.concatenate([jnp.broadcast_to(row[r + 4 : r + 5], (64, 128)) + col_ref[1] for r in range(4)], axis=0)

    def turned(values, gain):
        square = values * values
        lo = jnp.sum(jnp.where(low, square, 0.0), axis=1, keepdims=True)
        hi = jnp.sum(jnp.where(low, 0.0, square), axis=1, keepdims=True)
        mean = jnp.where(low, lo, hi) * (1.0 / 64.0)
        values = values * lax.rsqrt(mean + EPS) * gain
        other = jnp.where(swap_up, pltpu.roll(values, 112, 1), pltpu.roll(values, 16, 1))
        return values * cos + other * sin

    def eye(n):
        return (
            lax.broadcasted_iota(jnp.int32, (n, n), 0) == lax.broadcasted_iota(jnp.int32, (n, n), 1)
        ).astype(F32).astype(BF16)

    kv = jnp.concatenate([k_ref[...], v_ref[...]], axis=1).astype(F32)
    kv = jnp.where(low, turned(kv, gains_ref[1:2]), kv).astype(BF16)
    kv_t = nt(eye(128), kv).astype(BF16)
    docs = jnp.broadcast_to(doc_ref[...], (16, 256))
    same = lax.broadcasted_iota(jnp.int32, (16, 256), 0) == docs
    kt[z, y, c, 0:64, :] = kv_t[:64]
    kt[z, y, c, 64:80, :] = jnp.where(same, NEG, 0.0).astype(BF16)
    vt[z, y, c] = kv_t[64:]

    pl.semaphore_wait(barrier, 8)

    def send(part, key, held, link):
        n = index[part][key]
        ref = arrays[part]
        slot = ref.at[wz(held[0]), wy(held[1]), c]
        i = names.index(part)
        which = 0 if n < 28 else 1
        return pltpu.make_async_remote_copy(
            src_ref=slot,
            dst_ref=slot,
            send_sem=send_sem.at[i, which],
            recv_sem=recv_sem.at[i, n],
            device_id=neighbour[link],
            device_id_type=MESH,
        )

    def wait_recv(part, key):
        n = index[part][key]
        i = names.index(part)
        slot = arrays[part].at[wz(key[0]), wy(key[1]), c]
        pltpu.make_async_remote_copy(
            src_ref=slot,
            dst_ref=slot,
            send_sem=send_sem.at[i, 0],
            recv_sem=recv_sem.at[i, n],
            device_id=sibling,
            device_id_type=MESH,
        ).wait_recv()

    def to_sibling(part, dz, cc):
        i = names.index(part)
        slots = arrays[part].at[wz(dz), :, cc]
        return pltpu.make_async_remote_copy(
            src_ref=slots,
            dst_ref=slots,
            send_sem=sib_send.at[i, DZS.index(dz)],
            recv_sem=sib_recv.at[i, DZS.index(dz)],
            device_id=sibling,
            device_id_type=MESH,
        )

    def half(member):
        return ow.at[member, pl.ds(pl.multiple_of(128 * c, 128), 128)]

    def ow_copy(member, n, who):
        return pltpu.make_async_remote_copy(
            src_ref=half(member),
            dst_ref=half(member),
            send_sem=ow_send.at[n],
            recv_sem=ow_recv.at[n],
            device_id=who,
            device_id_type=MESH,
        )

    def other_half(member, mine):
        cc = c if mine else 1 - c
        return ow.at[member, pl.ds(pl.multiple_of(128 * cc, 128), 128)]

    def ow_sib(member, n, mine):
        ref = other_half(member, mine)
        return pltpu.make_async_remote_copy(
            src_ref=ref,
            dst_ref=ref,
            send_sem=ow_sib_send.at[n],
            recv_sem=ow_sib_recv.at[n],
            device_id=sibling,
            device_id_type=MESH,
        )

    def att_copy(member, n, who):
        return pltpu.make_async_remote_copy(
            src_ref=att.at[member],
            dst_ref=att.at[member],
            send_sem=att_send.at[n],
            recv_sem=att_recv.at[n],
            device_id=who,
            device_id_type=MESH,
        )

    def rs_copy(j, member, n, who):
        return pltpu.make_async_remote_copy(
            src_ref=part_buf.at[j, member],
            dst_ref=rs_buf.at[j, n],
            send_sem=rs_send.at[j, n],
            recv_sem=rs_recv.at[j, n],
            device_id=who,
            device_id_type=MESH,
        )

    def out_chunk(member, dz):
        return out_ref.at[member, :, pl.ds(pl.multiple_of(256 * wz(dz), 256), 256)]

    def ag_copy(t, member, n, who):
        ref = out_chunk(member, DZS[t])
        return pltpu.make_async_remote_copy(
            src_ref=ref,
            dst_ref=ref,
            send_sem=ag_send.at[t, n],
            recv_sem=ag_recv.at[t, n],
            device_id=who,
            device_id_type=MESH,
        )

    def more():
        local[2].wait()
        ow_copy(x, 0, x_f).start()
        ow_copy(x, 1, x_r).start()
        no = jnp.where(same, 0.0, 1.0).astype(BF16)
        no = jnp.concatenate([jnp.zeros((64, 256), BF16), no, jnp.zeros((48, 256), BF16)], axis=0)
        no_t = nt(eye(256), no)
        for pair in range(2):
            both = turned(q_ref[:, 128 * pair : 128 * pair + 128].astype(F32), gains_ref[0:1]) * 0.125
            for odd in range(2):
                head = pltpu.roll(both, 64, 1) if odd else both
                qs[2 * pair + odd] = jnp.where(low, head, no_t).astype(BF16)
        m_ref[...] = jnp.full((4, 256, 128), NEG, F32)
        l_ref[...] = jnp.zeros((4, 256, 128), F32)
        acc_ref[...] = jnp.zeros((4, 256, 64), F32)
        down_t = nt(eye(32), down_ref[...]).astype(BF16)
        wa[z, y, c] = down_t[:, :1152]
        wb[z, y, c] = down_t[:, 1152:]

    def ow_forward():
        ow_copy(wx(-d), 0, x_f).wait_recv()
        ow_copy(wx(-d), 2, x_f).start()
        ow_sib(wx(-d), 0, True).start()
        ow_copy(wx(d), 1, x_r).wait_recv()
        ow_sib(wx(d), 1, True).start()

    def ow_last():
        ow_copy(wx(2), 2, x_f).wait_recv()
        ow_sib(wx(2), 2, True).start()

    def ow_wait():
        ow_sib(wx(d), 0, False).wait_recv()
        ow_sib(wx(-d), 1, False).wait_recv()
        ow_sib(wx(2), 2, False).wait_recv()

    def attend(dz, own):
        zz = wz(dz)
        cc = c if own else 1 - c

        def head(h, carry):
            q = qs[h][:, :80]
            for j in range(4):
                s_ref[:, 256 * j : 256 * j + 256] = nn(q, kt[zz, j, cc])
            for r in range(0, 256, 64):
                rows = slice(r, r + 64)
                sc = s_ref[rows, :]
                old = m_ref[h, rows, :]
                new = jnp.maximum(old, jnp.max(sc, axis=1, keepdims=True))
                shrink = jnp.exp(old - new)
                m_ref[h, rows, :] = new
                w = jnp.exp(sc - new[:, :1])
                part = w[:, :128]
                for t in range(1, 8):
                    part = part + w[:, 128 * t : 128 * t + 128]
                l_ref[h, rows, :] = l_ref[h, rows, :] * shrink + part
                acc_ref[h, rows, :] = acc_ref[h, rows, :] * shrink[:, :64]
                p_ref[rows, :] = w.astype(BF16)
            pv = nt(p_ref[:, 0:256], vt[zz, 0, cc])
            for j in range(1, 4):
                pv = pv + nt(p_ref[:, 256 * j : 256 * j + 256], vt[zz, j, cc])
            acc_ref[h] = acc_ref[h] + pv
            return carry

        lax.fori_loop(0, 4, head, 0)

    def attended():
        pieces = []
        for h in range(4):
            total = jnp.sum(l_ref[h], axis=1, keepdims=True)
            pieces.append(acc_ref[h] / total)
        att[x] = jnp.concatenate(pieces, axis=1).astype(BF16)
        att_copy(x, 0, x_f).start()
        att_copy(x, 1, x_r).start()

    def mix(n):
        if n == 0:
            att_copy(wx(2), 2, x_f).wait_recv()
            ow_wait()
            local[3].wait()
        rows = slice(128 * n, 128 * n + 128)
        total = tok[rows, :].astype(F32)
        mixed = jnp.zeros((128, 2048), F32)
        for member in range(4):
            mixed = mixed + nn(att[member, rows, :], ow[member]).astype(BF16).astype(F32)
        total = total + mixed
        resid[2 * n] = total[:64]
        resid[2 * n + 1] = total[64:]
        mean = jnp.mean(total * total, axis=1, keepdims=True)
        scaled = (total * lax.rsqrt(mean + EPS) * ng_ref[...]).astype(BF16)
        for t in range(8):
            normed[t, rows, :] = scaled[:, 256 * t : 256 * t + 256]

    def gateup(n):
        cols = slice(256 * n, min(256 * n + 256, 1408))
        width = cols.stop - cols.start
        gate = jnp.zeros((256, width), F32)
        up = jnp.zeros((256, width), F32)
        for t in range(8):
            a = normed[t]
            gate = gate + nn(a, wg[t, :, :, :, cols].reshape(256, width))
            up = up + nn(a, wu[t, :, :, :, cols].reshape(256, width))
        hidden[:, cols] = (gate / (1.0 + jnp.exp(-gate)) * up).astype(BF16)

    def down(j):
        for t in range(2):
            zz = wz(DZS[2 * j + t])
            fed = nt(hidden[:, :1152], wa[zz].reshape(256, 1152)) + nt(hidden[:, 1152:], wb[zz].reshape(256, 256))
            fed = fed.astype(BF16)
            for member in range(4):
                part_buf[j, member, :, 256 * t : 256 * t + 256] = fed[64 * member : 64 * member + 64]
        rs_copy(j, wx(2), 2, x_far).start()
        rs_copy(j, wx(1), 0, x_plus).start()
        rs_copy(j, wx(-1), 1, x_minus).start()

    def reduce(j):
        rs_copy(j, wx(1), 0, x_plus).wait_recv()
        rs_copy(j, wx(-1), 1, x_minus).wait_recv()
        rs_copy(j, wx(2), 2, x_far).wait_recv()
        total = part_buf[j, x].astype(F32)
        for n in range(3):
            total = total + rs_buf[j, n].astype(F32)
        for t in range(2):
            zz = wz(DZS[2 * j + t])
            cols = pl.ds(pl.multiple_of(256 * zz, 256), 256)
            out_ref[x, :, cols] = (resid[x, :, cols] + total[:, 256 * t : 256 * t + 256]).astype(BF16)
            ag_copy(2 * j + t, x, 0, x_f).start()
            ag_copy(2 * j + t, x, 1, x_r).start()

    def relay(j):
        for t in (2 * j, 2 * j + 1):
            ag_copy(t, wx(-d), 0, x_f).wait_recv()
            ag_copy(t, wx(-d), 2, x_f).start()

    def end():
        for i, name in enumerate(names):
            ref = arrays[name]
            many = ref.at[0:7, :, 0]
            few = ref.at[0, 0:3, 0]
            pltpu.make_async_remote_copy(
                src_ref=many,
                dst_ref=many,
                send_sem=send_sem.at[i, 0],
                recv_sem=recv_sem.at[i, 0],
                device_id=sibling,
                device_id_type=MESH,
            ).wait_send()
            pltpu.make_async_remote_copy(
                src_ref=few,
                dst_ref=few,
                send_sem=send_sem.at[i, 1],
                recv_sem=recv_sem.at[i, 0],
                device_id=sibling,
                device_id_type=MESH,
            ).wait_send()
            for dz in DZS:
                to_sibling(name, dz, c).wait_send()
        ow_copy(x, 0, x_f).wait_send()
        ow_copy(x, 1, x_r).wait_send()
        ow_copy(wx(-d), 2, x_f).wait_send()
        for n, member in enumerate((wx(-d), wx(d), wx(2))):
            ow_sib(member, n, True).wait_send()
        att_copy(x, 0, x_f).wait_send()
        att_copy(x, 1, x_r).wait_send()
        att_copy(wx(-d), 2, x_f).wait_send()
        for j in range(4):
            rs_copy(j, wx(2), 2, x_far).wait_send()
            rs_copy(j, wx(1), 0, x_plus).wait_send()
            rs_copy(j, wx(-1), 1, x_minus).wait_send()
        for t in range(8):
            ag_copy(t, wx(d), 1, x_r).wait_recv()
            ag_copy(t, wx(2), 2, x_f).wait_recv()
            ag_copy(t, x, 0, x_f).wait_send()
            ag_copy(t, x, 1, x_r).wait_send()
            ag_copy(t, wx(-d), 2, x_f).wait_send()

    order, _, _ = plan()
    local_left = True
    groups = 0
    for event in order:
        kind = event[0]
        if kind == "send":
            _, part, key, held, link = event
            if part in "gu" and local_left:
                local[0].wait()
                local[1].wait()
                local_left = False
            send(part, key, held, link).start()
        elif kind == "wait":
            wait_recv(event[1], event[2])
        elif kind == "sib":
            to_sibling(event[1], event[2], c).start()
        elif kind == "waitsib":
            to_sibling(event[1], event[2], 1 - c).wait_recv()
        elif kind == "more":
            more()
        elif kind == "attend":
            attend(event[1], event[2])
            groups += 1
            if groups == 7:
                ow_forward()
            if groups == 14:
                ow_last()
        elif kind == "attended":
            attended()
        elif kind == "x_att":
            att_copy(wx(-d), 0, x_f).wait_recv()
            att_copy(wx(-d), 2, x_f).start()
            att_copy(wx(d), 1, x_r).wait_recv()
        elif kind == "mix":
            mix(event[1])
        elif kind == "gateup":
            gateup(event[1])
        elif kind == "down":
            j = event[1]
            down(j)
            if j >= 1:
                reduce(j - 1)
            if j >= 2:
                relay(j - 2)
        elif kind == "end":
            reduce(3)
            relay(2)
            relay(3)
            end()


def per_device(
    tokens_in,
    queries,
    keys,
    values,
    doc_ids,
    query_gain,
    key_norm_scale,
    out_weight,
    norm_gain,
    gate_weight,
    up_weight,
    down_weight,
):
    row, col = turn_tables()
    gains = jnp.stack([jnp.tile(query_gain, 2), jnp.tile(key_norm_scale, 2)])
    vmem = pl.BlockSpec(memory_space=pltpu.VMEM)
    hbm = pl.BlockSpec(memory_space=pl.ANY)
    dma = pltpu.SemaphoreType.DMA
    out = pl.pallas_call(
        kernel,
        name="layer",
        out_shape=jax.ShapeDtypeStruct((4, 64, 2048), BF16),
        in_specs=[hbm, vmem, vmem, vmem, vmem, vmem, hbm, vmem, hbm, hbm, vmem, vmem, vmem],
        out_specs=vmem,
        scratch_shapes=[
            pltpu.VMEM((NZ, NY, NC, 80, 256), BF16),
            pltpu.VMEM((NZ, NY, NC, 64, 256), BF16),
            pltpu.VMEM((NZ, NY, NC, 32, 1408), BF16),
            pltpu.VMEM((NZ, NY, NC, 32, 1408), BF16),
            pltpu.VMEM((NZ, NY, NC, 32, 1152), BF16),
            pltpu.VMEM((NZ, NY, NC, 32, 256), BF16),
            pltpu.VMEM((4, 256, 2048), BF16),
            pltpu.VMEM((4, 256, 256), BF16),
            pltpu.VMEM((4, 256, 128), BF16),
            pltpu.VMEM((4, 256, 128), F32),
            pltpu.VMEM((4, 256, 128), F32),
            pltpu.VMEM((4, 256, 64), F32),
            pltpu.VMEM((256, 1024), F32),
            pltpu.VMEM((256, 1024), BF16),
            pltpu.VMEM((256, 2048), BF16),
            pltpu.VMEM((4, 64, 2048), F32),
            pltpu.VMEM((8, 256, 256), BF16),
            pltpu.VMEM((256, 1408), BF16),
            pltpu.VMEM((4, 4, 64, 512), BF16),
            pltpu.VMEM((4, 3, 64, 512), BF16),
            dma((6, 31)),
            dma((6, 2)),
            dma((6, 8)),
            dma((6, 8)),
            dma((3,)),
            dma((3,)),
            dma((3,)),
            dma((3,)),
            dma((3,)),
            dma((3,)),
            dma((4, 3)),
            dma((4, 3)),
            dma((8, 3)),
            dma((8, 3)),
            dma((4,)),
        ],
        compiler_params=pltpu.CompilerParams(
            collective_id=0, has_side_effects=True, vmem_limit_bytes=60 * 1024 * 1024
        ),
    )(
        tokens_in,
        queries,
        keys,
        values,
        doc_ids.reshape(1, -1),
        gains,
        out_weight,
        norm_gain.reshape(1, -1),
        gate_weight,
        up_weight,
        down_weight,
        jnp.asarray(row),
        jnp.asarray(col),
    )
    return out.reshape(256, 2048)


def solution(mesh):
    return jax.shard_map(
        per_device,
        mesh=mesh,
        in_specs=(
            P("sp", None),
            P("sp", "tp"),
            P("sp", "tp"),
            P("sp", "tp"),
            P("sp"),
            P(),
            P(),
            P("tp", None),
            P(),
            P("sp", "tp"),
            P("sp", "tp"),
            P("tp", "sp"),
        ),
        out_specs=P("sp", None),
        check_vma=False,
    )
```

time: 339 us -> 131 us (0.39); the launches traced: 335 us -> 130 us
  blocking collectives: 164 us -> 0 us
  Pallas kernels: 0 us -> 123 us
  waiting for transfers between devices: 45.8 us -> 0 us
  loops' own time: 40.4 us -> 0 us
  local copies, waits for them, and re-layouts: 34.1 us -> 6.86 us
  matrix products: 23.6 us -> 0 us
  between operations: 13.3 us -> 0.02 us
  other arithmetic: 13.2 us -> 0.6 us
    pallas_call x0 -> x1, Pallas kernels: none -> 123 us  [per_device(): pl.pallas_call(kernel, name='layer', out_shape=jax.ShapeDtypeStruct((4, 6...]
    all_to_all x2 -> x0, blocking collectives: 100 us -> none  [sent_to_all(): return lax.all_to_all(copies, axis, split_axis=0, concat_axis=0, tiled=True)]
    all_gather x1 -> x0, blocking collectives: 63.4 us -> none  [per_device(): lax.all_gather(doc_pairs, 'sp', axis=0, tiled=True)]
    all_gather x3 -> x0, waiting for transfers between devices: 45.1 us -> none  [the longest x1 35 us: per_device(): lax.all_gather(down_weight, 'sp', axis=1, tiled=True)]
    another operation x17 -> x0, loops' own time: 40.4 us -> none  [the longest x1 40.1 us: per_device(): lax.scan(visit, carry, (key_blocks, value_blocks, doc_blocks))]
    dot_general x7 -> x0, matrix products: 23.6 us -> none  [the longest x1 9.48 us: per_device(): jnp.dot(hidden, lax.all_gather(down_weight, 'sp', axis=1, tiled=True), pr...]
    reshape x6 -> x0, local copies, waits for them, and re-layouts: 14.5 us -> none  [the longest x1 6.12 us: per_device(): key_blocks = key_piece.reshape(blocks, span_rows, head_dim)]
    slice x17 -> x0, local copies, waits for them, and re-layouts: 10.2 us -> none  [the longest x16 9.5 us: absorb_block(): touches = (doc_block[0] <= last_doc) & (doc_block[-1] >= first_doc)]
  transfers between devices with their start and end apart: 3 -> 0, of which waited for: 2 -> 0; matrix products, arithmetic and copies ran while one was open for 16% -> 0% of each run, Pallas kernels for 0% -> 0%
where the time goes in v1:
time: 131 us; the launch traced here: 130 us
  Pallas kernels  123 us (94%)
  local copies, waits for them, and re-layouts  6.86 us (5%)
    pallas_call x1, Pallas kernels, per_device(): pl.pallas_call(kernel, name='layer', out_shape=jax.ShapeDtypeStruct((4, 6...  123 us
    unnamed x12, local copies, waits for them, and re-layouts  6.69 us

profile of v1, /device:TPU:1, one launch (start us, length us, event | category | flops | bytes accessed | tf_op | source)
XLA Modules:
  0.0 130.5 jit_solution(4349550078111450395)
XLA Ops:
  0.0 0.0 copy-start.2
  0.0 0.7 copy-done.2
  0.7 0.0 copy-start.3
  0.7 0.1 stack_tile.6
  0.7 0.6 copy-done.3
  1.3 0.1 stack_tile.7
  1.4 0.0 copy-start.1
  1.4 0.6 pad_maximum_fusion.gains_ref
  2.0 0.0 copy-start
  2.0 1.5 %copy.15.k_ref = bf16[256,64]{1,0:T(8,128)(2,1)} copy(bf16[256,64]{0,1:T(8,128)(2,1)} %param.16) | data formatting | bytes 65536 | tf_op args[2]
  3.5 0.0 copy-done.1
  3.5 0.7 copy.16.v_ref
  4.2 0.0 copy-done
  4.2 0.9 copy.17.down_ref
  5.2 123.0 %layer.1 = bf16[4,64,2048]{2,1,0:T(8,128)(2,1)} custom-call(bf16[256,2048]{1,0:T(8,128)(2,1)} %tokens_ref.1, bf16[256,256]{1,0:T(8,128)(2,1)} %q_ref.1, bf16[256,64]{1,0:T(8,128)(2,1)} %copy.15.k_ref, bf16[256,64]{1,0:T(8,128)(2,1)} %copy.16.v_ref, s32[1,256]{1,0:T(1,128)} %bitcast.5, f32[2,128]{1,0:T(2,128)} %pad_maximum_fusion.gains_ref, ...), custom_call_target="tpu_custom_call" | custom-call | tf_op jit(solution)/shard_map/layer/pallas_call | solution.py:652
  128.2 2.3 %copy.19 = bf16[256,2048]{1,0:T(8,128)(2,1)} copy(bf16[256,2048]{1,0:T(8,128)(2,1)} %bitcast.3) | data formatting | bytes 2097152
  (2 shorter events, 0.0 us)
Async XLA Ops:
  0.0 0.7 copy-start.2
  0.7 0.7 copy-start.3
  1.4 2.1 %copy-start.1 = (bf16[256,64]{0,1:T(8,128)(2,1)S(1)}, bf16[256,64]{0,1:T(8,128)(2,1)}, u32[]{:S(2)}) copy-start(bf16[256,64]{0,1:T(8,128)(2,1)} %param.17) | copy-start | bytes 98308
  2.0 2.2 %copy-start = (bf16[1408,32]{0,1:T(8,128)(2,1)S(1)}, bf16[1408,32]{0,1:T(8,128)(2,1)}, u32[]{:S(2)}) copy-start(bf16[1408,32]{0,1:T(8,128)(2,1)} %param.25) | copy-start | bytes 270340

commit v2 on v1

--- a/solution.py
+++ b/solution.py
@@ -17,14 +17,18 @@
 MESH = pl.DeviceIdType.MESH
 F32, BF16 = jnp.float32, jnp.bfloat16
 
+DOWN_A = 768
 PARTS = (
-    ("k", "zy", 0.88, 0),
-    ("v", "yz", 0.70, 0),
-    ("g", "zy", 1.93, 1),
-    ("u", "yz", 1.93, 1),
-    ("a", "zy", 1.58, 2),
-    ("b", "yz", 0.35, 2),
+    ("k", "zy", 1, 0.88, -37.1),
+    ("v", "yz", 0, 0.70, 19.9),
+    ("g", "zy", 1, 1.93, 78.0),
+    ("u", "yz", 0, 1.93, 73.8),
+    ("a", "zy", 0, 1.93 * 6 / 11, 96.9),
+    ("b", "yz", 0, 1.93 * 5 / 11, 101.0),
 )
+HOP = 4.4
+BACKLOG = 2.0
+LATENCY = 2.4
 
 
 def spread(order, flip):
@@ -53,9 +57,10 @@
 
 
 def plan():
-    received = {p[0]: spread(p[1], i % 2) for i, p in enumerate(PARTS)}
-    cost = {p[0]: p[2] for p in PARTS}
-    prio = {p[0]: p[3] for p in PARTS}
+    received = {p[0]: spread(p[1], p[2]) for p in PARTS}
+    cost = {p[0]: p[3] for p in PARTS}
+    due = {p[0]: p[4] for p in PARTS}
+    times = {"attend": 2.0, "attended": 0.4, "mix": 1.0, "gateup": 0.78, "down": 0.4, "reduce": 0.2}
     follow = {}
     for part, messages in received.items():
         for key, (link, held) in messages.items():
@@ -64,85 +69,112 @@
     def depth(part, key):
         return max([1 + depth(part, k) for _, k in follow.get((part, key), [])], default=0)
 
-    now, order = 0.0, []
-    link_free = {link: 0.0 for link in ("z+", "z-", "y+", "y-", "d")}
-    queues = {link: [] for link in link_free}
+    now, count, order = 0.0, 0, []
+    link_free = {link: 0.0 for link in ("z+", "z-", "y+", "y-", "d", "x")}
+    queues = {link: [] for link in ("z+", "z-", "y+", "y-")}
     arrivals = []
-    have, sib = set(), set()
-    latency, count = 2.0, 0
+    have, sib, done = set(), set(), set()
+
+    def push(when, *event):
+        nonlocal count
+        count += 1
+        heapq.heappush(arrivals, (when, count) + event)
 
     def got(part, key):
         nonlocal count
         have.add((part, key))
         for link, k in follow.get((part, key), []):
             count += 1
-            heapq.heappush(queues[link], (prio[part], -depth(part, k), count, part, k, key))
+            heapq.heappush(queues[link], (due[part] - depth(part, k) * (cost[part] + HOP), count, part, k, key))
         dz = key[0]
         if all((part, (dz, dy)) in have for dy in DYS):
             order.append(("sib", part, dz))
             start = max(now, link_free["d"])
             link_free["d"] = start + 0.3
-            count += 1
-            heapq.heappush(arrivals, (start + 1.5, count, "sib", part, dz))
+            push(start + 1.5, "sib", part, dz)
 
     def tick():
-        nonlocal count
         while arrivals and arrivals[0][0] <= now:
             _, _, kind, part, key = heapq.heappop(arrivals)
             order.append(("wait" + kind, part, key))
             if kind == "sib":
                 sib.add((part, key))
+            elif kind == "":
+                got(part, key)
             else:
-                got(part, key)
-        for link in ("z+", "z-", "y+", "y-"):
-            q = queues[link]
-            while q and link_free[link] - now < 3.0:
-                _, _, _, part, key, held = heapq.heappop(q)
+                done.add((kind, part))
+        for link, queue in queues.items():
+            while queue and link_free[link] - now < BACKLOG:
+                _, _, part, key, held = heapq.heappop(queue)
                 order.append(("send", part, key, held, link))
-                start = max(now, link_free[link])
-                link_free[link] = start + cost[part]
-                count += 1
-                heapq.heappush(arrivals, (link_free[link] + latency, count, "", part, key))
+                link_free[link] = max(now, link_free[link]) + cost[part]
+                push(link_free[link] + LATENCY, "", part, key)
+
+    def near(parts, dz):
+        return all((p, (dz, dy)) in have for p in parts for dy in DYS)
 
     def ready(step):
         kind = step[0]
         if kind == "attend":
-            _, dz, own = step
-            return all(((p, (dz, dy)) in have for p in "kv" for dy in DYS) if own else ((p, dz) in sib for p in "kv"))
+            return near("kv", step[1]) if step[2] else all((p, step[1]) in sib for p in "kv")
         if kind == "gateup":
-            return all((p, (dz, dy)) in have for p in "gu" for dz in DZS for dy in DYS) and all(
-                (p, dz) in sib for p in "gu" for dz in DZS
-            )
+            return all(near("gu", dz) and all((p, dz) in sib for p in "gu") for dz in DZS)
+        if kind == "mix":
+            return ("att", 0) in done
         if kind == "down":
-            return all(
-                all((p, (dz, dy)) in have for p in "ab" for dy in DYS) and all((p, dz) in sib for p in "ab")
-                for dz in DZS[2 * step[1] : 2 * step[1] + 2]
-            )
+            return near("ab", step[1]) and all((p, step[1]) in sib for p in "ab")
+        if kind == "reduce":
+            return ("rs", step[1]) in done
         return True
 
-    steps = [("attend", dz, own) for dz in DZS for own in (True, False)]
-    times = {"attend": 2.2, "attended": 1.0, "x_att": 2.5, "x_att2": 2.5, "mix": 1.0, "gateup": 0.9, "down": 0.8}
-    steps += [("attended",), ("x_att",), ("x_att2",), ("mix", 0), ("mix", 1)]
-    steps += [("gateup", n) for n in range(6)]
-    steps += [("down", n) for n in range(4)]
+    def run(step):
+        nonlocal now
+        order.append(step)
+        now += times[step[0]]
+        sends = {"attended": ("att", 5.0), "down": ("rs", 1.4), "reduce": ("ag", 1.4)}
+        if step[0] in sends:
+            kind, length = sends[step[0]]
+            link_free["x"] = max(now, link_free["x"]) + length
+            push(link_free["x"] + LATENCY, kind, step[1], 0)
+
+    def advance():
+        nonlocal now
+        now = max(now, arrivals[0][0])
+        tick()
+
     for part in "kvgu":
         got(part, (0, 0))
     tick()
     order.append(("more",))
     for part in "ab":
         got(part, (0, 0))
+    now = 0.75
+    steps = [("attend", dz, own) for dz in DZS for own in (True, False)]
+    steps += [("attended", 0), ("mix", 0), ("mix", 1)]
+    steps += [("gateup", n) for n in range(6)]
     for step in steps:
         tick()
         while not ready(step):
-            now = max(now, arrivals[0][0])
-            tick()
-        order.append(step)
-        now += times[step[0]]
+            advance()
+        run(step)
+    downs, reduces = list(DZS), []
+    while downs or reduces:
+        tick()
+        steps = [("reduce", dz) for dz in reduces] + [("down", dz) for dz in downs]
+        step = next((step for step in steps if ready(step)), None)
+        if step is None:
+            advance()
+            continue
+        run(step)
+        if step[0] == "down":
+            downs.remove(step[1])
+            reduces.append(step[1])
+        else:
+            reduces.remove(step[1])
     while arrivals:
-        now = max(now, arrivals[0][0])
-        tick()
+        advance()
     order.append(("end",))
-    return order, now, link_free
+    return order, now
 
 
 def turn_tables():
@@ -175,7 +207,8 @@
     k_ref,
     v_ref,
     doc_ref,
-    gains_ref,
+    qg_ref,
+    kg_ref,
     ow_ref,
     ng_ref,
     gate_ref,
@@ -225,7 +258,6 @@
     c = lax.rem(s, NC)
     y = lax.rem(s // NC, NY)
     z = s // (NC * NY)
-    d = 1 - 2 * c
 
     def wz(dz):
         return lax.rem(z + (dz + NZ), NZ)
@@ -249,19 +281,20 @@
     x_plus = at(z, y, c, wx(1))
     x_minus = at(z, y, c, wx(-1))
     x_far = at(z, y, c, wx(2))
-    x_f = at(z, y, c, wx(d))
-    x_r = at(z, y, c, wx(-d))
 
     arrays = {"k": kt, "v": vt, "g": wg, "u": wu, "a": wa, "b": wb}
     names = [p[0] for p in PARTS]
-    received = {p[0]: spread(p[1], i % 2) for i, p in enumerate(PARTS)}
+    received = {p[0]: spread(p[1], p[2]) for p in PARTS}
     index = {name: {key: n for n, key in enumerate(received[name])} for name in names}
 
     local = [
-        pltpu.make_async_copy(gate_ref, wg.at[z, y, c], local_sem.at[0]),
-        pltpu.make_async_copy(up_ref, wu.at[z, y, c], local_sem.at[1]),
-        pltpu.make_async_copy(ow_ref, ow.at[x], local_sem.at[2]),
-        pltpu.make_async_copy(tokens_ref, tok, local_sem.at[3]),
+        pltpu.make_async_copy(v_ref, vt.at[z, y, c], local_sem.at[0]),
+        pltpu.make_async_copy(gate_ref, wg.at[z, y, c], local_sem.at[1]),
+        pltpu.make_async_copy(up_ref, wu.at[z, y, c], local_sem.at[2]),
+        pltpu.make_async_copy(down_ref.at[:, :DOWN_A], wa.at[z, y, c], local_sem.at[3]),
+        pltpu.make_async_copy(down_ref.at[:, DOWN_A:], wb.at[z, y, c], local_sem.at[4]),
+        pltpu.make_async_copy(ow_ref, ow.at[x], local_sem.at[5]),
+        pltpu.make_async_copy(tokens_ref, tok, local_sem.at[6]),
     ]
     for copy in local:
         copy.start()
@@ -291,14 +324,18 @@
             lax.broadcasted_iota(jnp.int32, (n, n), 0) == lax.broadcasted_iota(jnp.int32, (n, n), 1)
         ).astype(F32).astype(BF16)
 
-    kv = jnp.concatenate([k_ref[...], v_ref[...]], axis=1).astype(F32)
-    kv = jnp.where(low, turned(kv, gains_ref[1:2]), kv).astype(BF16)
-    kv_t = nt(eye(128), kv).astype(BF16)
+    keys = k_ref[...].astype(F32)
+    gain = jnp.where(
+        lax.broadcasted_iota(jnp.int32, (64, 64), 0) == lax.broadcasted_iota(jnp.int32, (64, 64), 1), kg_ref[...], 0.0
+    )
+    keys = keys * lax.rsqrt(jnp.mean(keys * keys, axis=0, keepdims=True) + EPS) * jnp.sum(gain, axis=1, keepdims=True)
+    other = jnp.concatenate([keys[16:32], keys[0:16], keys[48:64], keys[32:48]], axis=0)
+    keys = keys * jnp.transpose(cos)[:64] + other * jnp.transpose(sin)[:64]
     docs = jnp.broadcast_to(doc_ref[...], (16, 256))
     same = lax.broadcasted_iota(jnp.int32, (16, 256), 0) == docs
-    kt[z, y, c, 0:64, :] = kv_t[:64]
+    kt[z, y, c, 0:64, :] = keys.astype(BF16)
     kt[z, y, c, 64:80, :] = jnp.where(same, NEG, 0.0).astype(BF16)
-    vt[z, y, c] = kv_t[64:]
+    local[0].wait()
 
     pl.semaphore_wait(barrier, 8)
 
@@ -405,51 +442,51 @@
         )
 
     def more():
-        local[2].wait()
-        ow_copy(x, 0, x_f).start()
-        ow_copy(x, 1, x_r).start()
+        local[5].wait()
+        ow_copy(x, 2, x_far).start()
+        ow_copy(x, 0, x_plus).start()
+        ow_copy(x, 1, x_minus).start()
         no = jnp.where(same, 0.0, 1.0).astype(BF16)
         no = jnp.concatenate([jnp.zeros((64, 256), BF16), no, jnp.zeros((48, 256), BF16)], axis=0)
         no_t = nt(eye(256), no)
+        query_gain = jnp.concatenate([qg_ref[...], qg_ref[...]], axis=1)
         for pair in range(2):
-            both = turned(q_ref[:, 128 * pair : 128 * pair + 128].astype(F32), gains_ref[0:1]) * 0.125
+            both = turned(q_ref[:, 128 * pair : 128 * pair + 128].astype(F32), query_gain) * 0.125
             for odd in range(2):
                 head = pltpu.roll(both, 64, 1) if odd else both
                 qs[2 * pair + odd] = jnp.where(low, head, no_t).astype(BF16)
         m_ref[...] = jnp.full((4, 256, 128), NEG, F32)
         l_ref[...] = jnp.zeros((4, 256, 128), F32)
         acc_ref[...] = jnp.zeros((4, 256, 64), F32)
-        down_t = nt(eye(32), down_ref[...]).astype(BF16)
-        wa[z, y, c] = down_t[:, :1152]
-        wb[z, y, c] = down_t[:, 1152:]
+        local[3].wait()
+        local[4].wait()
 
     def ow_forward():
-        ow_copy(wx(-d), 0, x_f).wait_recv()
-        ow_copy(wx(-d), 2, x_f).start()
-        ow_sib(wx(-d), 0, True).start()
-        ow_copy(wx(d), 1, x_r).wait_recv()
-        ow_sib(wx(d), 1, True).start()
-
-    def ow_last():
-        ow_copy(wx(2), 2, x_f).wait_recv()
-        ow_sib(wx(2), 2, True).start()
+        for n, member in enumerate((wx(-1), wx(1), wx(2))):
+            ow_copy(member, n, x_far).wait_recv()
+            ow_sib(member, n, True).start()
 
     def ow_wait():
-        ow_sib(wx(d), 0, False).wait_recv()
-        ow_sib(wx(-d), 1, False).wait_recv()
-        ow_sib(wx(2), 2, False).wait_recv()
-
-    def attend(dz, own):
-        zz = wz(dz)
-        cc = c if own else 1 - c
-
-        def head(h, carry):
+        for n, member in enumerate((wx(-1), wx(1), wx(2))):
+            ow_sib(member, n, False).wait_recv()
+
+    def attend(i):
+        n = i // 2
+        zz = wz((n + 1) // 2 * (2 * lax.rem(n, 2) - 1))
+        cc = lax.rem(c + i, 2)
+
+        def scores(h):
             q = qs[h][:, :80]
             for j in range(4):
-                s_ref[:, 256 * j : 256 * j + 256] = nn(q, kt[zz, j, cc])
-            for r in range(0, 256, 64):
-                rows = slice(r, r + 64)
-                sc = s_ref[rows, :]
+                s_ref[h % 2, :, 256 * j : 256 * j + 256] = nn(q, kt[zz, j, cc])
+
+        scores(0)
+        for h in range(4):
+            if h < 3:
+                scores(h + 1)
+            for r in range(0, 256, 32):
+                rows = slice(r, r + 32)
+                sc = s_ref[h % 2, rows, :]
                 old = m_ref[h, rows, :]
                 new = jnp.maximum(old, jnp.max(sc, axis=1, keepdims=True))
                 shrink = jnp.exp(old - new)
@@ -460,14 +497,11 @@
                     part = part + w[:, 128 * t : 128 * t + 128]
                 l_ref[h, rows, :] = l_ref[h, rows, :] * shrink + part
                 acc_ref[h, rows, :] = acc_ref[h, rows, :] * shrink[:, :64]
-                p_ref[rows, :] = w.astype(BF16)
-            pv = nt(p_ref[:, 0:256], vt[zz, 0, cc])
+                p_ref[h % 2, rows, :] = w.astype(BF16)
+            pv = nt(p_ref[h % 2, :, 0:256], vt[zz, 0, cc])
             for j in range(1, 4):
-                pv = pv + nt(p_ref[:, 256 * j : 256 * j + 256], vt[zz, j, cc])
+                pv = pv + nt(p_ref[h % 2, :, 256 * j : 256 * j + 256], vt[zz, j, cc])
             acc_ref[h] = acc_ref[h] + pv
-            return carry
-
-        lax.fori_loop(0, 4, head, 0)
 
     def attended():
         pieces = []
@@ -475,14 +509,14 @@
             total = jnp.sum(l_ref[h], axis=1, keepdims=True)
             pieces.append(acc_ref[h] / total)
         att[x] = jnp.concatenate(pieces, axis=1).astype(BF16)
-        att_copy(x, 0, x_f).start()
-        att_copy(x, 1, x_r).start()
+        att_copy(x, 2, x_far).start()
+        att_copy(x, 0, x_plus).start()
+        att_copy(x, 1, x_minus).start()
 
     def mix(n):
         if n == 0:
-            att_copy(wx(2), 2, x_f).wait_recv()
             ow_wait()
-            local[3].wait()
+            local[6].wait()
         rows = slice(128 * n, 128 * n + 128)
         total = tok[rows, :].astype(F32)
         mixed = jnp.zeros((128, 2048), F32)
@@ -507,35 +541,37 @@
             up = up + nn(a, wu[t, :, :, :, cols].reshape(256, width))
         hidden[:, cols] = (gate / (1.0 + jnp.exp(-gate)) * up).astype(BF16)
 
-    def down(j):
-        for t in range(2):
-            zz = wz(DZS[2 * j + t])
-            fed = nt(hidden[:, :1152], wa[zz].reshape(256, 1152)) + nt(hidden[:, 1152:], wb[zz].reshape(256, 256))
-            fed = fed.astype(BF16)
-            for member in range(4):
-                part_buf[j, member, :, 256 * t : 256 * t + 256] = fed[64 * member : 64 * member + 64]
+    def down(dz):
+        j = DZS.index(dz)
+        zz = wz(dz)
+        fed = nt(hidden[:, :DOWN_A], wa[zz].reshape(256, DOWN_A))
+        fed = (fed + nt(hidden[:, DOWN_A:], wb[zz].reshape(256, 1408 - DOWN_A))).astype(BF16)
+        for member in range(4):
+            part_buf[j, member] = fed[64 * member : 64 * member + 64]
         rs_copy(j, wx(2), 2, x_far).start()
         rs_copy(j, wx(1), 0, x_plus).start()
         rs_copy(j, wx(-1), 1, x_minus).start()
 
-    def reduce(j):
-        rs_copy(j, wx(1), 0, x_plus).wait_recv()
-        rs_copy(j, wx(-1), 1, x_minus).wait_recv()
-        rs_copy(j, wx(2), 2, x_far).wait_recv()
+    def wait_rs(dz):
+        j = DZS.index(dz)
+        for n in range(3):
+            rs_copy(j, x, n, x_far).wait_recv()
+
+    def reduce(dz):
+        j = DZS.index(dz)
         total = part_buf[j, x].astype(F32)
         for n in range(3):
             total = total + rs_buf[j, n].astype(F32)
-        for t in range(2):
-            zz = wz(DZS[2 * j + t])
-            cols = pl.ds(pl.multiple_of(256 * zz, 256), 256)
-            out_ref[x, :, cols] = (resid[x, :, cols] + total[:, 256 * t : 256 * t + 256]).astype(BF16)
-            ag_copy(2 * j + t, x, 0, x_f).start()
-            ag_copy(2 * j + t, x, 1, x_r).start()
-
-    def relay(j):
-        for t in (2 * j, 2 * j + 1):
-            ag_copy(t, wx(-d), 0, x_f).wait_recv()
-            ag_copy(t, wx(-d), 2, x_f).start()
+        cols = pl.ds(pl.multiple_of(256 * wz(dz), 256), 256)
+        out_ref[x, :, cols] = (resid[x, :, cols] + total).astype(BF16)
+        ag_copy(j, x, 2, x_far).start()
+        ag_copy(j, x, 0, x_plus).start()
+        ag_copy(j, x, 1, x_minus).start()
+
+    def wait_ag(dz):
+        j = DZS.index(dz)
+        for n, member in enumerate((wx(-1), wx(1), wx(2))):
+            ag_copy(j, member, n, x_far).wait_recv()
 
     def end():
         for i, name in enumerate(names):
@@ -560,36 +596,25 @@
             ).wait_send()
             for dz in DZS:
                 to_sibling(name, dz, c).wait_send()
-        ow_copy(x, 0, x_f).wait_send()
-        ow_copy(x, 1, x_r).wait_send()
-        ow_copy(wx(-d), 2, x_f).wait_send()
-        for n, member in enumerate((wx(-d), wx(d), wx(2))):
+        for n, who in enumerate((x_plus, x_minus, x_far)):
+            ow_copy(x, n, who).wait_send()
+            att_copy(x, n, who).wait_send()
+        for n, member in enumerate((wx(-1), wx(1), wx(2))):
             ow_sib(member, n, True).wait_send()
-        att_copy(x, 0, x_f).wait_send()
-        att_copy(x, 1, x_r).wait_send()
-        att_copy(wx(-d), 2, x_f).wait_send()
-        for j in range(4):
-            rs_copy(j, wx(2), 2, x_far).wait_send()
-            rs_copy(j, wx(1), 0, x_plus).wait_send()
-            rs_copy(j, wx(-1), 1, x_minus).wait_send()
-        for t in range(8):
-            ag_copy(t, wx(d), 1, x_r).wait_recv()
-            ag_copy(t, wx(2), 2, x_f).wait_recv()
-            ag_copy(t, x, 0, x_f).wait_send()
-            ag_copy(t, x, 1, x_r).wait_send()
-            ag_copy(t, wx(-d), 2, x_f).wait_send()
-
-    order, _, _ = plan()
-    local_left = True
-    groups = 0
-    for event in order:
+        for j in range(8):
+            for n, (who, member) in enumerate(((x_plus, wx(1)), (x_minus, wx(-1)), (x_far, wx(2)))):
+                rs_copy(j, member, n, who).wait_send()
+                ag_copy(j, x, n, who).wait_send()
+
+    done = set()
+
+    def handle(event):
         kind = event[0]
         if kind == "send":
             _, part, key, held, link = event
-            if part in "gu" and local_left:
-                local[0].wait()
-                local[1].wait()
-                local_left = False
+            if part in "gu" and part not in done:
+                local[1 + "gu".index(part)].wait()
+                done.add(part)
             send(part, key, held, link).start()
         elif kind == "wait":
             wait_recv(event[1], event[2])
@@ -599,35 +624,48 @@
             to_sibling(event[1], event[2], 1 - c).wait_recv()
         elif kind == "more":
             more()
-        elif kind == "attend":
-            attend(event[1], event[2])
-            groups += 1
-            if groups == 7:
-                ow_forward()
-            if groups == 14:
-                ow_last()
         elif kind == "attended":
             attended()
-        elif kind == "x_att":
-            att_copy(wx(-d), 0, x_f).wait_recv()
-            att_copy(wx(-d), 2, x_f).start()
-            att_copy(wx(d), 1, x_r).wait_recv()
+        elif kind == "waitatt":
+            for n, member in enumerate((wx(-1), wx(1), wx(2))):
+                att_copy(member, n, x_far).wait_recv()
         elif kind == "mix":
             mix(event[1])
         elif kind == "gateup":
             gateup(event[1])
         elif kind == "down":
-            j = event[1]
-            down(j)
-            if j >= 1:
-                reduce(j - 1)
-            if j >= 2:
-                relay(j - 2)
+            down(event[1])
+        elif kind == "waitrs":
+            wait_rs(event[1])
+        elif kind == "reduce":
+            reduce(event[1])
+        elif kind == "waitag":
+            wait_ag(event[1])
         elif kind == "end":
-            reduce(3)
-            relay(2)
-            relay(3)
             end()
+
+    order, _ = plan()
+    attends = [n for n, event in enumerate(order) if event[0] == "attend"]
+    for event in order[: attends[0]]:
+        handle(event)
+
+    def step(i, carry):
+        attend(i)
+        for n in range(16):
+            stop = attends[n + 1] if n < 15 else attends[15] + 1
+
+            @pl.when(i == n)
+            def _():
+                for event in order[attends[n] + 1 : stop]:
+                    handle(event)
+                if n == 11:
+                    ow_forward()
+
+        return carry
+
+    lax.fori_loop(0, 16, step, 0)
+    for event in order[attends[15] + 1 :]:
+        handle(event)
 
 
 def per_device(
@@ -645,7 +683,6 @@
     down_weight,
 ):
     row, col = turn_tables()
-    gains = jnp.stack([jnp.tile(query_gain, 2), jnp.tile(key_norm_scale, 2)])
     vmem = pl.BlockSpec(memory_space=pltpu.VMEM)
     hbm = pl.BlockSpec(memory_space=pl.ANY)
     dma = pltpu.SemaphoreType.DMA
@@ -653,29 +690,29 @@
         kernel,
         name="layer",
         out_shape=jax.ShapeDtypeStruct((4, 64, 2048), BF16),
-        in_specs=[hbm, vmem, vmem, vmem, vmem, vmem, hbm, vmem, hbm, hbm, vmem, vmem, vmem],
+        in_specs=[hbm, vmem, vmem, hbm, vmem, vmem, vmem, hbm, vmem, hbm, hbm, hbm, vmem, vmem],
         out_specs=vmem,
         scratch_shapes=[
             pltpu.VMEM((NZ, NY, NC, 80, 256), BF16),
             pltpu.VMEM((NZ, NY, NC, 64, 256), BF16),
             pltpu.VMEM((NZ, NY, NC, 32, 1408), BF16),
             pltpu.VMEM((NZ, NY, NC, 32, 1408), BF16),
-            pltpu.VMEM((NZ, NY, NC, 32, 1152), BF16),
-            pltpu.VMEM((NZ, NY, NC, 32, 256), BF16),
+            pltpu.VMEM((NZ, NY, NC, 32, DOWN_A), BF16),
+            pltpu.VMEM((NZ, NY, NC, 32, 1408 - DOWN_A), BF16),
             pltpu.VMEM((4, 256, 2048), BF16),
             pltpu.VMEM((4, 256, 256), BF16),
             pltpu.VMEM((4, 256, 128), BF16),
             pltpu.VMEM((4, 256, 128), F32),
             pltpu.VMEM((4, 256, 128), F32),
             pltpu.VMEM((4, 256, 64), F32),
-            pltpu.VMEM((256, 1024), F32),
-            pltpu.VMEM((256, 1024), BF16),
+            pltpu.VMEM((2, 256, 1024), F32),
+            pltpu.VMEM((2, 256, 1024), BF16),
             pltpu.VMEM((256, 2048), BF16),
             pltpu.VMEM((4, 64, 2048), F32),
             pltpu.VMEM((8, 256, 256), BF16),
             pltpu.VMEM((256, 1408), BF16),
-            pltpu.VMEM((4, 4, 64, 512), BF16),
-            pltpu.VMEM((4, 3, 64, 512), BF16),
+            pltpu.VMEM((8, 4, 64, 256), BF16),
+            pltpu.VMEM((8, 3, 64, 256), BF16),
             dma((6, 31)),
             dma((6, 2)),
             dma((6, 8)),
@@ -686,11 +723,11 @@
             dma((3,)),
             dma((3,)),
             dma((3,)),
-            dma((4, 3)),
-            dma((4, 3)),
             dma((8, 3)),
             dma((8, 3)),
-            dma((4,)),
+            dma((8, 3)),
+            dma((8, 3)),
+            dma((7,)),
         ],
         compiler_params=pltpu.CompilerParams(
             collective_id=0, has_side_effects=True, vmem_limit_bytes=60 * 1024 * 1024
@@ -698,15 +735,16 @@
     )(
         tokens_in,
         queries,
-        keys,
-        values,
+        keys.T,
+        values.T,
         doc_ids.reshape(1, -1),
-        gains,
+        query_gain.reshape(1, -1),
+        key_norm_scale.reshape(1, -1),
         out_weight,
         norm_gain.reshape(1, -1),
         gate_weight,
         up_weight,
-        down_weight,
+        down_weight.T,
         jnp.asarray(row),
         jnp.asarray(col),
     )

time: 131 us -> 102 us (0.78)
  Pallas kernels: 123 us -> 100 us
  local copies, waits for them, and re-layouts: 6.86 us -> 2.3 us
    pallas_call x1, Pallas kernels: 123 us -> 100 us  [per_device(): pl.pallas_call(kernel, name='layer', out_shape=jax.ShapeDtypeStruct((4, 6...]
    unnamed x12 -> x1, local copies, waits for them, and re-layouts: 6.69 us -> 2.3 us
where the time goes in v2:
time: 102 us
  Pallas kernels  100 us (98%)
  local copies, waits for them, and re-layouts  2.3 us (2%)
    pallas_call x1, Pallas kernels, per_device(): pl.pallas_call(kernel, name='layer', out_shape=jax.ShapeDtypeStruct((4, 6...  100 us
    unnamed x1, local copies, waits for them, and re-layouts  2.3 us

profile of v2, /device:TPU:1, one launch (start us, length us, event | category | flops | bytes accessed | tf_op | source)
XLA Modules:
  0.0 102.3 jit_solution(11523753327365648231)
XLA Ops:
  0.0 100.0 %layer.1 = bf16[4,64,2048]{2,1,0:T(8,128)(2,1)} custom-call(bf16[256,2048]{1,0:T(8,128)(2,1)} %tokens_ref.1, bf16[256,256]{1,0:T(8,128)(2,1)} %q_ref.1, bf16[64,256]{1,0:T(8,128)(2,1)} %bitcast.10, bf16[64,256]{1,0:T(8,128)(2,1)} %bitcast.11, s32[1,256]{1,0:T(1,128)} %bitcast.13, f32[1,64]{1,0:T(1,128)} %bitcast.14, f32[1,64]{1,0:T(1,128)} %bitcast.15, ...), custom_call_target="tpu_custom_call" | custom-call | tf_op jit(solution)/shard_map/layer/pallas_call | solution.py:689
  100.0 2.3 %copy.16 = bf16[256,2048]{1,0:T(8,128)(2,1)} copy(bf16[256,2048]{1,0:T(8,128)(2,1)} %bitcast.8) | data formatting | bytes 2097152

commit v3 on v2

--- a/solution.py
+++ b/solution.py
@@ -19,16 +19,16 @@
 
 DOWN_A = 768
 PARTS = (
-    ("k", "zy", 1, 0.88, -37.1),
-    ("v", "yz", 0, 0.70, 19.9),
-    ("g", "zy", 1, 1.93, 78.0),
-    ("u", "yz", 0, 1.93, 73.8),
-    ("a", "zy", 0, 1.93 * 6 / 11, 96.9),
-    ("b", "yz", 0, 1.93 * 5 / 11, 101.0),
+    ("k", "zy", 0, 0.88, 19.3),
+    ("v", "yz", 1, 0.70, 3.1),
+    ("g", "zy", 1, 1.93, 44.4),
+    ("u", "yz", 0, 1.93, 57.4),
+    ("a", "zy", 0, 1.93 * 6 / 11, 74.5),
+    ("b", "yz", 1, 1.93 * 5 / 11, 91.7),
 )
-HOP = 4.4
+HOP = 4.9
 BACKLOG = 2.0
-LATENCY = 2.4
+LATENCY = 2.9
 
 
 def spread(order, flip):
@@ -60,7 +60,7 @@
     received = {p[0]: spread(p[1], p[2]) for p in PARTS}
     cost = {p[0]: p[3] for p in PARTS}
     due = {p[0]: p[4] for p in PARTS}
-    times = {"attend": 2.0, "attended": 0.4, "mix": 1.0, "gateup": 0.78, "down": 0.4, "reduce": 0.2}
+    times = {"first": 2.1, "attend": 2.1, "half": 1.15, "pair": 0.25, "attended": 1.2, "mix": 0.7, "norm": 0.6, "gateup": 0.78, "down": 0.4, "reduce": 0.2}
     follow = {}
     for part, messages in received.items():
         for key, (link, held) in messages.items():
@@ -87,11 +87,15 @@
             count += 1
             heapq.heappush(queues[link], (due[part] - depth(part, k) * (cost[part] + HOP), count, part, k, key))
         dz = key[0]
-        if all((part, (dz, dy)) in have for dy in DYS):
+        if part in "kv" and dz == 0:
+            order.append(("one", part, key[1]))
+            link_free["d"] = max(now, link_free["d"]) + 0.1
+            push(link_free["d"] + 1.7, "one", part, key[1])
+        elif all((part, (dz, dy)) in have for dy in DYS):
             order.append(("sib", part, dz))
             start = max(now, link_free["d"])
             link_free["d"] = start + 0.3
-            push(start + 1.5, "sib", part, dz)
+            push(start + 2.0, "sib", part, dz)
 
     def tick():
         while arrivals and arrivals[0][0] <= now:
@@ -101,6 +105,8 @@
                 sib.add((part, key))
             elif kind == "":
                 got(part, key)
+            elif kind == "one":
+                done.add((kind, part, key))
             else:
                 done.add((kind, part))
         for link, queue in queues.items():
@@ -115,12 +121,14 @@
 
     def ready(step):
         kind = step[0]
-        if kind == "attend":
+        if kind == "first":
+            return near("kv", 0) and all(("one", p, dy) in done for p in "kv" for dy in step[1:])
+        if kind in ("attend", "half"):
             return near("kv", step[1]) if step[2] else all((p, step[1]) in sib for p in "kv")
         if kind == "gateup":
             return all(near("gu", dz) and all((p, dz) in sib for p in "gu") for dz in DZS)
         if kind == "mix":
-            return ("att", 0) in done
+            return ("att", step[1]) in done
         if kind == "down":
             return near("ab", step[1]) and all((p, step[1]) in sib for p in "ab")
         if kind == "reduce":
@@ -131,11 +139,14 @@
         nonlocal now
         order.append(step)
         now += times[step[0]]
-        sends = {"attended": ("att", 5.0), "down": ("rs", 1.4), "reduce": ("ag", 1.4)}
-        if step[0] in sends:
-            kind, length = sends[step[0]]
-            link_free["x"] = max(now, link_free["x"]) + length
-            push(link_free["x"] + LATENCY, kind, step[1], 0)
+        if step[0] == "pair":
+            link_free["x"] = now + 2.8
+        if step[0] == "attended":
+            for n, length in enumerate((1.4, 1.5, 2.8)):
+                push(max(now - 0.8, link_free["x"]) + length + LATENCY, "att", n, 0)
+        if step[0] == "down":
+            link_free["x"] = max(now, link_free["x"]) + 1.4
+            push(link_free["x"] + LATENCY, "rs", step[1], 0)
 
     def advance():
         nonlocal now
@@ -149,8 +160,13 @@
     for part in "ab":
         got(part, (0, 0))
     now = 0.75
-    steps = [("attend", dz, own) for dz in DZS for own in (True, False)]
-    steps += [("attended", 0), ("mix", 0), ("mix", 1)]
+    steps = [("first", 0, 1), ("first", -1, 2), ("attend", DZS[1], True)]
+    for n in range(1, 7):
+        steps += [("attend", DZS[n + 1], True), ("attend", DZS[n], False)]
+    steps.append(("attend", DZS[7], False))
+    halves = [("half", *step[1:]) for step in steps[12:]]
+    steps = steps[:12] + halves + [("pair", 0)] + halves + [("attended", 0)]
+    steps += [("mix", 0), ("mix", 1), ("mix", 2), ("norm", 0)]
     steps += [("gateup", n) for n in range(6)]
     for step in steps:
         tick()
@@ -237,6 +253,7 @@
     hidden,
     part_buf,
     rs_buf,
+    mine,
     recv_sem,
     send_sem,
     sib_recv,
@@ -252,6 +269,8 @@
     ag_recv,
     ag_send,
     local_sem,
+    drain_sem,
+    one_recv,
 ):
     s = lax.axis_index("sp")
     x = lax.axis_index("tp")
@@ -259,14 +278,10 @@
     y = lax.rem(s // NC, NY)
     z = s // (NC * NY)
 
-    def wz(dz):
-        return lax.rem(z + (dz + NZ), NZ)
-
-    def wy(dy):
-        return lax.rem(y + (dy + NY), NY)
-
-    def wx(dx):
-        return lax.rem(x + (dx + NX), NX)
+    z_at = {dz: lax.rem(z + (dz + NZ), NZ) for dz in DZS}
+    y_at = {dy: lax.rem(y + (dy + NY), NY) for dy in DYS}
+    x_at = {dx: lax.rem(x + (dx + NX), NX) for dx in DYS}
+    wz, wy, wx = z_at.__getitem__, y_at.__getitem__, x_at.__getitem__
 
     def at(zz, yy, cc, xx):
         return ((zz * NY + yy) * NC + cc, xx)
@@ -373,11 +388,34 @@
         return pltpu.make_async_remote_copy(
             src_ref=slots,
             dst_ref=slots,
-            send_sem=sib_send.at[i, DZS.index(dz)],
+            send_sem=sib_send.at[i],
             recv_sem=sib_recv.at[i, DZS.index(dz)],
             device_id=sibling,
             device_id_type=MESH,
         )
+
+    def one_to_sibling(part, dy, cc):
+        i = names.index(part)
+        slot = arrays[part].at[z, wy(dy), cc]
+        return pltpu.make_async_remote_copy(
+            src_ref=slot,
+            dst_ref=slot,
+            send_sem=sib_send.at[i],
+            recv_sem=one_recv.at[i, DYS.index(dy)],
+            device_id=sibling,
+            device_id_type=MESH,
+        )
+
+    def together(ref, send=None, recv=None):
+        copy = pltpu.make_async_remote_copy(
+            src_ref=ref,
+            dst_ref=ref,
+            send_sem=drain_sem.at[0] if send is None else send,
+            recv_sem=drain_sem.at[0] if recv is None else recv,
+            device_id=sibling,
+            device_id_type=MESH,
+        )
+        copy.wait_send() if send is not None else copy.wait_recv()
 
     def half(member):
         return ow.at[member, pl.ds(pl.multiple_of(128 * c, 128), 128)]
@@ -386,8 +424,8 @@
         return pltpu.make_async_remote_copy(
             src_ref=half(member),
             dst_ref=half(member),
-            send_sem=ow_send.at[n],
-            recv_sem=ow_recv.at[n],
+            send_sem=ow_send.at[0],
+            recv_sem=ow_recv.at[0],
             device_id=who,
             device_id_type=MESH,
         )
@@ -401,17 +439,17 @@
         return pltpu.make_async_remote_copy(
             src_ref=ref,
             dst_ref=ref,
-            send_sem=ow_sib_send.at[n],
-            recv_sem=ow_sib_recv.at[n],
+            send_sem=ow_sib_send.at[0],
+            recv_sem=ow_sib_recv.at[0],
             device_id=sibling,
             device_id_type=MESH,
         )
 
-    def att_copy(member, n, who):
+    def att_copy(member, pair, n, who):
         return pltpu.make_async_remote_copy(
-            src_ref=att.at[member],
-            dst_ref=att.at[member],
-            send_sem=att_send.at[n],
+            src_ref=att.at[member, pair],
+            dst_ref=att.at[member, pair],
+            send_sem=att_send.at[0],
             recv_sem=att_recv.at[n],
             device_id=who,
             device_id_type=MESH,
@@ -421,22 +459,21 @@
         return pltpu.make_async_remote_copy(
             src_ref=part_buf.at[j, member],
             dst_ref=rs_buf.at[j, n],
-            send_sem=rs_send.at[j, n],
-            recv_sem=rs_recv.at[j, n],
+            send_sem=rs_send.at[0],
+            recv_sem=rs_recv.at[j],
             device_id=who,
             device_id_type=MESH,
         )
 
-    def out_chunk(member, dz):
-        return out_ref.at[member, :, pl.ds(pl.multiple_of(256 * wz(dz), 256), 256)]
-
-    def ag_copy(t, member, n, who):
-        ref = out_chunk(member, DZS[t])
+    def out_chunk(dz):
+        return out_ref.at[x, :, pl.ds(pl.multiple_of(256 * wz(dz), 256), 256)]
+
+    def ag_copy(j, who):
         return pltpu.make_async_remote_copy(
-            src_ref=ref,
-            dst_ref=ref,
-            send_sem=ag_send.at[t, n],
-            recv_sem=ag_recv.at[t, n],
+            src_ref=mine.at[j],
+            dst_ref=out_chunk(DZS[j]),
+            send_sem=ag_send.at[0],
+            recv_sem=ag_recv.at[0],
             device_id=who,
             device_id_type=MESH,
         )
@@ -462,31 +499,39 @@
         local[4].wait()
 
     def ow_forward():
+        together(ow.at[0:3, 0:128], recv=ow_recv.at[0])
         for n, member in enumerate((wx(-1), wx(1), wx(2))):
-            ow_copy(member, n, x_far).wait_recv()
             ow_sib(member, n, True).start()
 
     def ow_wait():
-        for n, member in enumerate((wx(-1), wx(1), wx(2))):
-            ow_sib(member, n, False).wait_recv()
-
-    def attend(i):
-        n = i // 2
-        zz = wz((n + 1) // 2 * (2 * lax.rem(n, 2) - 1))
-        cc = lax.rem(c + i, 2)
-
-        def scores(h):
-            q = qs[h][:, :80]
+        together(ow.at[0:3, 0:128], recv=ow_sib_recv.at[0])
+
+    def attend(i, heads):
+        e0, e1, e2, e15 = (1 // (1 + (i - k) * (i - k)) for k in (0, 1, 2, 15))
+        odd, start = lax.rem(i, 2), e0 + e1
+        far = odd * ((i + 1) // 2) + (1 - odd) * (i // 2 - 1) + e0 - e1 + e2 - e15
+        zz = lax.rem(z + NZ + (far + 1) // 2 * (2 * lax.rem(far, 2) - 1), NZ)
+        cc = lax.rem(c + 1 - odd - e2 + e15, 2)
+        pieces = [
+            (
+                start * lax.rem(y + 2 * i + j // 2, NY) + (1 - start) * j,
+                start * (j % 2) + (1 - start) * cc,
+            )
+            for j in range(4)
+        ]
+
+        def scores(n):
+            q = qs[heads[n]][:, :80]
             for j in range(4):
-                s_ref[h % 2, :, 256 * j : 256 * j + 256] = nn(q, kt[zz, j, cc])
+                s_ref[n % 2, :, 256 * j : 256 * j + 256] = nn(q, kt[zz, pieces[j][0], pieces[j][1]])
 
         scores(0)
-        for h in range(4):
-            if h < 3:
-                scores(h + 1)
+        for n, h in enumerate(heads):
+            if n + 1 < len(heads):
+                scores(n + 1)
             for r in range(0, 256, 32):
                 rows = slice(r, r + 32)
-                sc = s_ref[h % 2, rows, :]
+                sc = s_ref[n % 2, rows, :]
                 old = m_ref[h, rows, :]
                 new = jnp.maximum(old, jnp.max(sc, axis=1, keepdims=True))
                 shrink = jnp.exp(old - new)
@@ -497,38 +542,48 @@
                     part = part + w[:, 128 * t : 128 * t + 128]
                 l_ref[h, rows, :] = l_ref[h, rows, :] * shrink + part
                 acc_ref[h, rows, :] = acc_ref[h, rows, :] * shrink[:, :64]
-                p_ref[h % 2, rows, :] = w.astype(BF16)
-            pv = nt(p_ref[h % 2, :, 0:256], vt[zz, 0, cc])
+                p_ref[n % 2, rows, :] = w.astype(BF16)
+            pv = nt(p_ref[n % 2, :, 0:256], vt[zz, pieces[0][0], pieces[0][1]])
             for j in range(1, 4):
-                pv = pv + nt(p_ref[h % 2, :, 256 * j : 256 * j + 256], vt[zz, j, cc])
+                pv = pv + nt(p_ref[n % 2, :, 256 * j : 256 * j + 256], vt[zz, pieces[j][0], pieces[j][1]])
             acc_ref[h] = acc_ref[h] + pv
 
-    def attended():
+    def add(n, member, start):
+        rows = slice(128 * n, 128 * n + 128)
+        share = nn(att[member, 0, rows, :], ow[member, 0:128, :]) + nn(att[member, 1, rows, :], ow[member, 128:256, :])
+        share = share.astype(BF16).astype(F32)
+        if start is None:
+            start = resid[2 * n : 2 * n + 2].reshape(128, 2048)
+        resid[2 * n : 2 * n + 2] = (start + share).reshape(2, 64, 2048)
+
+    def attended(pair):
         pieces = []
-        for h in range(4):
+        for h in (2 * pair, 2 * pair + 1):
             total = jnp.sum(l_ref[h], axis=1, keepdims=True)
             pieces.append(acc_ref[h] / total)
-        att[x] = jnp.concatenate(pieces, axis=1).astype(BF16)
-        att_copy(x, 2, x_far).start()
-        att_copy(x, 0, x_plus).start()
-        att_copy(x, 1, x_minus).start()
+        att[x, pair] = jnp.concatenate(pieces, axis=1).astype(BF16)
+        att_copy(x, pair, 0, x_plus).start()
+        att_copy(x, pair, 1, x_minus).start()
+        att_copy(x, pair, 2, x_far).start()
+
+    def own_share():
+        ow_wait()
+        local[6].wait()
+        for n in range(2):
+            rows = slice(128 * n, 128 * n + 128)
+            add(n, x, tok[rows, :].astype(F32))
 
     def mix(n):
-        if n == 0:
-            ow_wait()
-            local[6].wait()
-        rows = slice(128 * n, 128 * n + 128)
-        total = tok[rows, :].astype(F32)
-        mixed = jnp.zeros((128, 2048), F32)
-        for member in range(4):
-            mixed = mixed + nn(att[member, rows, :], ow[member]).astype(BF16).astype(F32)
-        total = total + mixed
-        resid[2 * n] = total[:64]
-        resid[2 * n + 1] = total[64:]
-        mean = jnp.mean(total * total, axis=1, keepdims=True)
-        scaled = (total * lax.rsqrt(mean + EPS) * ng_ref[...]).astype(BF16)
-        for t in range(8):
-            normed[t, rows, :] = scaled[:, 256 * t : 256 * t + 256]
+        for half_rows in range(2):
+            add(half_rows, wx((-1, 1, 2)[n]), None)
+
+    def norm():
+        for n in range(2):
+            total = resid[2 * n : 2 * n + 2].reshape(128, 2048)
+            mean = jnp.mean(total * total, axis=1, keepdims=True)
+            scaled = (total * lax.rsqrt(mean + EPS) * ng_ref[...]).astype(BF16)
+            for t in range(8):
+                normed[t, 128 * n : 128 * n + 128, :] = scaled[:, 256 * t : 256 * t + 256]
 
     def gateup(n):
         cols = slice(256 * n, min(256 * n + 256, 1408))
@@ -554,8 +609,7 @@
 
     def wait_rs(dz):
         j = DZS.index(dz)
-        for n in range(3):
-            rs_copy(j, x, n, x_far).wait_recv()
+        together(rs_buf.at[j], recv=rs_recv.at[j])
 
     def reduce(dz):
         j = DZS.index(dz)
@@ -563,15 +617,11 @@
         for n in range(3):
             total = total + rs_buf[j, n].astype(F32)
         cols = pl.ds(pl.multiple_of(256 * wz(dz), 256), 256)
-        out_ref[x, :, cols] = (resid[x, :, cols] + total).astype(BF16)
-        ag_copy(j, x, 2, x_far).start()
-        ag_copy(j, x, 0, x_plus).start()
-        ag_copy(j, x, 1, x_minus).start()
-
-    def wait_ag(dz):
-        j = DZS.index(dz)
-        for n, member in enumerate((wx(-1), wx(1), wx(2))):
-            ag_copy(j, member, n, x_far).wait_recv()
+        mine[j] = (resid[x, :, cols] + total).astype(BF16)
+        ag_copy(j, x_far).start()
+        ag_copy(j, x_plus).start()
+        ag_copy(j, x_minus).start()
+        pltpu.make_async_copy(mine.at[j], out_chunk(dz), drain_sem.at[1]).start()
 
     def end():
         for i, name in enumerate(names):
@@ -594,17 +644,22 @@
                 device_id=sibling,
                 device_id_type=MESH,
             ).wait_send()
-            for dz in DZS:
-                to_sibling(name, dz, c).wait_send()
-        for n, who in enumerate((x_plus, x_minus, x_far)):
-            ow_copy(x, n, who).wait_send()
-            att_copy(x, n, who).wait_send()
-        for n, member in enumerate((wx(-1), wx(1), wx(2))):
-            ow_sib(member, n, True).wait_send()
-        for j in range(8):
-            for n, (who, member) in enumerate(((x_plus, wx(1)), (x_minus, wx(-1)), (x_far, wx(2)))):
-                rs_copy(j, member, n, who).wait_send()
-                ag_copy(j, x, n, who).wait_send()
+            every = ref.at[:, :, c]
+            pltpu.make_async_remote_copy(
+                src_ref=every,
+                dst_ref=every,
+                send_sem=sib_send.at[i],
+                recv_sem=recv_sem.at[i, 0],
+                device_id=sibling,
+                device_id_type=MESH,
+            ).wait_send()
+        together(ow.at[0:3, 0:128], send=ow_send.at[0])
+        together(ow.at[0:3, 0:128], send=ow_sib_send.at[0])
+        together(att.at[0:3], send=att_send.at[0])
+        together(part_buf.at[0:6], send=rs_send.at[0])
+        together(part_buf.at[0:6], send=ag_send.at[0])
+        pltpu.make_async_copy(mine, mine, drain_sem.at[1]).wait()
+        together(part_buf.at[0:6], recv=ag_recv.at[0])
 
     done = set()
 
@@ -620,17 +675,25 @@
             wait_recv(event[1], event[2])
         elif kind == "sib":
             to_sibling(event[1], event[2], c).start()
+        elif kind == "one":
+            one_to_sibling(event[1], event[2], c).start()
+        elif kind == "waitone":
+            one_to_sibling(event[1], event[2], 1 - c).wait_recv()
         elif kind == "waitsib":
             to_sibling(event[1], event[2], 1 - c).wait_recv()
         elif kind == "more":
             more()
         elif kind == "attended":
-            attended()
+            attended(1)
+            own_share()
+        elif kind == "pair":
+            attended(0)
         elif kind == "waitatt":
-            for n, member in enumerate((wx(-1), wx(1), wx(2))):
-                att_copy(member, n, x_far).wait_recv()
+            together(att.at[wx((-1, 1, 2)[event[1]])], recv=att_recv.at[event[1]])
         elif kind == "mix":
             mix(event[1])
+        elif kind == "norm":
+            norm()
         elif kind == "gateup":
             gateup(event[1])
         elif kind == "down":
@@ -639,32 +702,39 @@
             wait_rs(event[1])
         elif kind == "reduce":
             reduce(event[1])
-        elif kind == "waitag":
-            wait_ag(event[1])
         elif kind == "end":
             end()
 
     order, _ = plan()
-    attends = [n for n, event in enumerate(order) if event[0] == "attend"]
+    attends = [n for n, event in enumerate(order) if event[0] in ("first", "attend", "half")]
+    attends.append(attends[-1] + 1)
     for event in order[: attends[0]]:
         handle(event)
 
-    def step(i, carry):
-        attend(i)
-        for n in range(16):
-            stop = attends[n + 1] if n < 15 else attends[15] + 1
+    def between(i, low, high):
+        for n in range(low, high):
 
             @pl.when(i == n)
             def _():
-                for event in order[attends[n] + 1 : stop]:
+                for event in order[attends[n] + 1 : attends[n + 1]]:
                     handle(event)
                 if n == 11:
                     ow_forward()
 
+    def step(i, carry):
+        attend(i, range(4))
+        between(i, 0, 12)
         return carry
 
-    lax.fori_loop(0, 16, step, 0)
-    for event in order[attends[15] + 1 :]:
+    def half_step(i, carry):
+        pair = (i - 12) // 4
+        attend(12 + lax.rem(i, 4), (2 * pair, 2 * pair + 1))
+        between(i, 12, 20)
+        return carry
+
+    lax.fori_loop(0, 12, step, 0)
+    lax.fori_loop(12, 20, half_step, 0)
+    for event in order[attends[-1] :]:
         handle(event)
 
 
@@ -684,14 +754,15 @@
 ):
     row, col = turn_tables()
     vmem = pl.BlockSpec(memory_space=pltpu.VMEM)
-    hbm = pl.BlockSpec(memory_space=pl.ANY)
+    anywhere = pl.BlockSpec(memory_space=pl.ANY)
+    hbm = pl.BlockSpec(memory_space=pltpu.HBM)
     dma = pltpu.SemaphoreType.DMA
     out = pl.pallas_call(
         kernel,
         name="layer",
         out_shape=jax.ShapeDtypeStruct((4, 64, 2048), BF16),
         in_specs=[hbm, vmem, vmem, hbm, vmem, vmem, vmem, hbm, vmem, hbm, hbm, hbm, vmem, vmem],
-        out_specs=vmem,
+        out_specs=anywhere,
         scratch_shapes=[
             pltpu.VMEM((NZ, NY, NC, 80, 256), BF16),
             pltpu.VMEM((NZ, NY, NC, 64, 256), BF16),
@@ -700,7 +771,7 @@
             pltpu.VMEM((NZ, NY, NC, 32, DOWN_A), BF16),
             pltpu.VMEM((NZ, NY, NC, 32, 1408 - DOWN_A), BF16),
             pltpu.VMEM((4, 256, 2048), BF16),
-            pltpu.VMEM((4, 256, 256), BF16),
+            pltpu.VMEM((4, 2, 256, 128), BF16),
             pltpu.VMEM((4, 256, 128), BF16),
             pltpu.VMEM((4, 256, 128), F32),
             pltpu.VMEM((4, 256, 128), F32),
@@ -713,21 +784,24 @@
             pltpu.VMEM((256, 1408), BF16),
             pltpu.VMEM((8, 4, 64, 256), BF16),
             pltpu.VMEM((8, 3, 64, 256), BF16),
+            pltpu.VMEM((8, 64, 256), BF16),
             dma((6, 31)),
             dma((6, 2)),
             dma((6, 8)),
-            dma((6, 8)),
+            dma((6,)),
+            dma((1,)),
+            dma((1,)),
+            dma((1,)),
+            dma((1,)),
             dma((3,)),
-            dma((3,)),
-            dma((3,)),
-            dma((3,)),
-            dma((3,)),
-            dma((3,)),
-            dma((8, 3)),
-            dma((8, 3)),
-            dma((8, 3)),
-            dma((8, 3)),
+            dma((1,)),
+            dma((8,)),
+            dma((1,)),
+            dma((1,)),
+            dma((1,)),
             dma((7,)),
+            dma((2,)),
+            dma((2, 4)),
         ],
         compiler_params=pltpu.CompilerParams(
             collective_id=0, has_side_effects=True, vmem_limit_bytes=60 * 1024 * 1024

time: 102 us -> 103 us (level)
  no operation moved by 1% of the time
where the time goes in v3:
time: 103 us
  Pallas kernels  101 us (98%)
  local copies, waits for them, and re-layouts  2.3 us (2%)
    pallas_call x1, Pallas kernels, per_device(): pl.pallas_call(kernel, name='layer', out_shape=jax.ShapeDtypeStruct((4, 6...  101 us
    unnamed x1, local copies, waits for them, and re-layouts  2.3 us

profile of v3, /device:TPU:1, one launch (start us, length us, event | category | flops | bytes accessed | tf_op | source)
XLA Modules:
  0.0 102.9 jit_solution(6577973324574348135)
XLA Ops:
  0.0 100.6 %layer.1 = bf16[4,64,2048]{2,1,0:T(8,128)(2,1)} custom-call(bf16[256,2048]{1,0:T(8,128)(2,1)} %tokens_ref.1, bf16[256,256]{1,0:T(8,128)(2,1)} %q_ref.1, bf16[64,256]{1,0:T(8,128)(2,1)} %bitcast.10, bf16[64,256]{1,0:T(8,128)(2,1)} %bitcast.11, s32[1,256]{1,0:T(1,128)} %bitcast.13, f32[1,64]{1,0:T(1,128)} %bitcast.14, f32[1,64]{1,0:T(1,128)} %bitcast.15, ...), custom_call_target="tpu_custom_call" | custom-call | tf_op jit(solution)/shard_map/layer/pallas_call | solution.py:760
  100.6 2.3 %copy.16 = bf16[256,2048]{1,0:T(8,128)(2,1)} copy(bf16[256,2048]{1,0:T(8,128)(2,1)} %bitcast.8) | data formatting | bytes 2097152

commit v4 on v3

--- a/solution.py
+++ b/solution.py
@@ -17,16 +17,16 @@
 MESH = pl.DeviceIdType.MESH
 F32, BF16 = jnp.float32, jnp.bfloat16
 
-DOWN_A = 768
+DOWN_A = 1024
 PARTS = (
-    ("k", "zy", 0, 0.88, 19.3),
-    ("v", "yz", 1, 0.70, 3.1),
-    ("g", "zy", 1, 1.93, 44.4),
-    ("u", "yz", 0, 1.93, 57.4),
-    ("a", "zy", 0, 1.93 * 6 / 11, 74.5),
-    ("b", "yz", 1, 1.93 * 5 / 11, 91.7),
+    ("k", "zy", 0, 0.88, 15.8),
+    ("v", "yz", 1, 0.70, 8.6),
+    ("g", "zy", 1, 1.93, 30.8),
+    ("u", "yz", 1, 1.93, 32.7),
+    ("a", "zy", 0, 1.93 * 8 / 11, 47.5),
+    ("b", "yz", 1, 1.93 * 3 / 11, 57.9),
 )
-HOP = 4.9
+HOP = 3.7
 BACKLOG = 2.0
 LATENCY = 2.9
 
@@ -60,7 +60,7 @@
     received = {p[0]: spread(p[1], p[2]) for p in PARTS}
     cost = {p[0]: p[3] for p in PARTS}
     due = {p[0]: p[4] for p in PARTS}
-    times = {"first": 2.1, "attend": 2.1, "half": 1.15, "pair": 0.25, "attended": 1.2, "mix": 0.7, "norm": 0.6, "gateup": 0.78, "down": 0.4, "reduce": 0.2}
+    times = {"first": 2.1, "attend": 2.1, "attended": 1.2, "mix": 0.7, "norm": 0.6, "gateup": 0.78, "down": 0.4, "reduce": 0.2}
     follow = {}
     for part, messages in received.items():
         for key, (link, held) in messages.items():
@@ -122,8 +122,8 @@
     def ready(step):
         kind = step[0]
         if kind == "first":
-            return near("kv", 0) and all(("one", p, dy) in done for p in "kv" for dy in step[1:])
-        if kind in ("attend", "half"):
+            return all((p, (0, dy)) in have and ("one", p, dy) in done for p in "kv" for dy in step[1:])
+        if kind == "attend":
             return near("kv", step[1]) if step[2] else all((p, step[1]) in sib for p in "kv")
         if kind == "gateup":
             return all(near("gu", dz) and all((p, dz) in sib for p in "gu") for dz in DZS)
@@ -139,11 +139,9 @@
         nonlocal now
         order.append(step)
         now += times[step[0]]
-        if step[0] == "pair":
-            link_free["x"] = now + 2.8
         if step[0] == "attended":
-            for n, length in enumerate((1.4, 1.5, 2.8)):
-                push(max(now - 0.8, link_free["x"]) + length + LATENCY, "att", n, 0)
+            for n, length in enumerate((2.8, 2.9, 5.5)):
+                push(now + length + LATENCY, "att", n, 0)
         if step[0] == "down":
             link_free["x"] = max(now, link_free["x"]) + 1.4
             push(link_free["x"] + LATENCY, "rs", step[1], 0)
@@ -163,10 +161,7 @@
     steps = [("first", 0, 1), ("first", -1, 2), ("attend", DZS[1], True)]
     for n in range(1, 7):
         steps += [("attend", DZS[n + 1], True), ("attend", DZS[n], False)]
-    steps.append(("attend", DZS[7], False))
-    halves = [("half", *step[1:]) for step in steps[12:]]
-    steps = steps[:12] + halves + [("pair", 0)] + halves + [("attended", 0)]
-    steps += [("mix", 0), ("mix", 1), ("mix", 2), ("norm", 0)]
+    steps += [("attend", DZS[7], False), ("attended", 0), ("mix", 0), ("mix", 1), ("mix", 2), ("norm", 0)]
     steps += [("gateup", n) for n in range(6)]
     for step in steps:
         tick()
@@ -445,10 +440,10 @@
             device_id_type=MESH,
         )
 
-    def att_copy(member, pair, n, who):
+    def att_copy(member, n, who):
         return pltpu.make_async_remote_copy(
-            src_ref=att.at[member, pair],
-            dst_ref=att.at[member, pair],
+            src_ref=att.at[member],
+            dst_ref=att.at[member],
             send_sem=att_send.at[0],
             recv_sem=att_recv.at[n],
             device_id=who,
@@ -506,11 +501,11 @@
     def ow_wait():
         together(ow.at[0:3, 0:128], recv=ow_sib_recv.at[0])
 
-    def attend(i, heads):
+    def attend(i):
         e0, e1, e2, e15 = (1 // (1 + (i - k) * (i - k)) for k in (0, 1, 2, 15))
         odd, start = lax.rem(i, 2), e0 + e1
-        far = odd * ((i + 1) // 2) + (1 - odd) * (i // 2 - 1) + e0 - e1 + e2 - e15
-        zz = lax.rem(z + NZ + (far + 1) // 2 * (2 * lax.rem(far, 2) - 1), NZ)
+        n = odd * ((i + 1) // 2) + (1 - odd) * (i // 2 - 1) + e0 - e1 + e2 - e15
+        zz = lax.rem(z + NZ + (n + 1) // 2 * (2 * lax.rem(n, 2) - 1), NZ)
         cc = lax.rem(c + 1 - odd - e2 + e15, 2)
         pieces = [
             (
@@ -520,18 +515,18 @@
             for j in range(4)
         ]
 
-        def scores(n):
-            q = qs[heads[n]][:, :80]
+        def scores(h):
+            q = qs[h][:, :80]
             for j in range(4):
-                s_ref[n % 2, :, 256 * j : 256 * j + 256] = nn(q, kt[zz, pieces[j][0], pieces[j][1]])
+                s_ref[h % 2, :, 256 * j : 256 * j + 256] = nn(q, kt[zz, pieces[j][0], pieces[j][1]])
 
         scores(0)
-        for n, h in enumerate(heads):
-            if n + 1 < len(heads):
-                scores(n + 1)
+        for h in range(4):
+            if h < 3:
+                scores(h + 1)
             for r in range(0, 256, 32):
                 rows = slice(r, r + 32)
-                sc = s_ref[n % 2, rows, :]
+                sc = s_ref[h % 2, rows, :]
                 old = m_ref[h, rows, :]
                 new = jnp.maximum(old, jnp.max(sc, axis=1, keepdims=True))
                 shrink = jnp.exp(old - new)
@@ -542,31 +537,27 @@
                     part = part + w[:, 128 * t : 128 * t + 128]
                 l_ref[h, rows, :] = l_ref[h, rows, :] * shrink + part
                 acc_ref[h, rows, :] = acc_ref[h, rows, :] * shrink[:, :64]
-                p_ref[n % 2, rows, :] = w.astype(BF16)
-            pv = nt(p_ref[n % 2, :, 0:256], vt[zz, pieces[0][0], pieces[0][1]])
+                p_ref[h % 2, rows, :] = w.astype(BF16)
+            pv = nt(p_ref[h % 2, :, 0:256], vt[zz, pieces[0][0], pieces[0][1]])
             for j in range(1, 4):
-                pv = pv + nt(p_ref[n % 2, :, 256 * j : 256 * j + 256], vt[zz, pieces[j][0], pieces[j][1]])
+                pv = pv + nt(p_ref[h % 2, :, 256 * j : 256 * j + 256], vt[zz, pieces[j][0], pieces[j][1]])
             acc_ref[h] = acc_ref[h] + pv
 
     def add(n, member, start):
-        rows = slice(128 * n, 128 * n + 128)
-        share = nn(att[member, 0, rows, :], ow[member, 0:128, :]) + nn(att[member, 1, rows, :], ow[member, 128:256, :])
-        share = share.astype(BF16).astype(F32)
+        share = nn(att[member, 128 * n : 128 * n + 128, :], ow[member]).astype(BF16).astype(F32)
         if start is None:
             start = resid[2 * n : 2 * n + 2].reshape(128, 2048)
         resid[2 * n : 2 * n + 2] = (start + share).reshape(2, 64, 2048)
 
-    def attended(pair):
+    def attended():
         pieces = []
-        for h in (2 * pair, 2 * pair + 1):
+        for h in range(4):
             total = jnp.sum(l_ref[h], axis=1, keepdims=True)
             pieces.append(acc_ref[h] / total)
-        att[x, pair] = jnp.concatenate(pieces, axis=1).astype(BF16)
-        att_copy(x, pair, 0, x_plus).start()
-        att_copy(x, pair, 1, x_minus).start()
-        att_copy(x, pair, 2, x_far).start()
-
-    def own_share():
+        att[x] = jnp.concatenate(pieces, axis=1).astype(BF16)
+        att_copy(x, 0, x_plus).start()
+        att_copy(x, 1, x_minus).start()
+        att_copy(x, 2, x_far).start()
         ow_wait()
         local[6].wait()
         for n in range(2):
@@ -684,12 +675,9 @@
         elif kind == "more":
             more()
         elif kind == "attended":
-            attended(1)
-            own_share()
-        elif kind == "pair":
-            attended(0)
+            attended()
         elif kind == "waitatt":
-            together(att.at[wx((-1, 1, 2)[event[1]])], recv=att_recv.at[event[1]])
+            att_copy(wx((-1, 1, 2)[event[1]]), event[1], x_far).wait_recv()
         elif kind == "mix":
             mix(event[1])
         elif kind == "norm":
@@ -706,35 +694,26 @@
             end()
 
     order, _ = plan()
-    attends = [n for n, event in enumerate(order) if event[0] in ("first", "attend", "half")]
-    attends.append(attends[-1] + 1)
+    attends = [n for n, event in enumerate(order) if event[0] in ("first", "attend")]
     for event in order[: attends[0]]:
         handle(event)
 
-    def between(i, low, high):
-        for n in range(low, high):
+    def step(i, carry):
+        attend(i)
+        for n in range(16):
+            stop = attends[n + 1] if n < 15 else attends[15] + 1
 
             @pl.when(i == n)
             def _():
-                for event in order[attends[n] + 1 : attends[n + 1]]:
+                for event in order[attends[n] + 1 : stop]:
                     handle(event)
                 if n == 11:
                     ow_forward()
 
-    def step(i, carry):
-        attend(i, range(4))
-        between(i, 0, 12)
         return carry
 
-    def half_step(i, carry):
-        pair = (i - 12) // 4
-        attend(12 + lax.rem(i, 4), (2 * pair, 2 * pair + 1))
-        between(i, 12, 20)
-        return carry
-
-    lax.fori_loop(0, 12, step, 0)
-    lax.fori_loop(12, 20, half_step, 0)
-    for event in order[attends[-1] :]:
+    lax.fori_loop(0, 16, step, 0)
+    for event in order[attends[15] + 1 :]:
         handle(event)
 
 
@@ -771,7 +750,7 @@
             pltpu.VMEM((NZ, NY, NC, 32, DOWN_A), BF16),
             pltpu.VMEM((NZ, NY, NC, 32, 1408 - DOWN_A), BF16),
             pltpu.VMEM((4, 256, 2048), BF16),
-            pltpu.VMEM((4, 2, 256, 128), BF16),
+            pltpu.VMEM((4, 256, 256), BF16),
             pltpu.VMEM((4, 256, 128), BF16),
             pltpu.VMEM((4, 256, 128), F32),
             pltpu.VMEM((4, 256, 128), F32),

time: 103 us -> 101 us (0.981)
  Pallas kernels: 101 us -> 98.5 us
    pallas_call x1, Pallas kernels: 101 us -> 98.5 us  [per_device(): pl.pallas_call(kernel, name='layer', out_shape=jax.ShapeDtypeStruct((4, 6...]
where the time goes in v4:
time: 101 us
  Pallas kernels  98.5 us (98%)
  local copies, waits for them, and re-layouts  2.3 us (2%)
    pallas_call x1, Pallas kernels, per_device(): pl.pallas_call(kernel, name='layer', out_shape=jax.ShapeDtypeStruct((4, 6...  98.5 us
    unnamed x1, local copies, waits for them, and re-layouts  2.3 us

profile of v4, /device:TPU:1, one launch (start us, length us, event | category | flops | bytes accessed | tf_op | source)
XLA Modules:
  0.0 100.8 jit_solution(17327208346475160239)
XLA Ops:
  0.0 98.5 %layer.1 = bf16[4,64,2048]{2,1,0:T(8,128)(2,1)} custom-call(bf16[256,2048]{1,0:T(8,128)(2,1)} %tokens_ref.1, bf16[256,256]{1,0:T(8,128)(2,1)} %q_ref.1, bf16[64,256]{1,0:T(8,128)(2,1)} %bitcast.10, bf16[64,256]{1,0:T(8,128)(2,1)} %bitcast.11, s32[1,256]{1,0:T(1,128)} %bitcast.13, f32[1,64]{1,0:T(1,128)} %bitcast.14, f32[1,64]{1,0:T(1,128)} %bitcast.15, ...), custom_call_target="tpu_custom_call" | custom-call | tf_op jit(solution)/shard_map/layer/pallas_call | solution.py:739
  98.5 2.3 %copy.16 = bf16[256,2048]{1,0:T(8,128)(2,1)} copy(bf16[256,2048]{1,0:T(8,128)(2,1)} %bitcast.8) | data formatting | bytes 2097152
